TPU v7x, 32 devices: a whole 2x2x4 slice. The times are simulated.
32 devices in a mesh: fs: 4 (over y, x), tp: 8 (over z, core).
Axes of the slice: x: 2, y: 2, z: 4, core: 2. Of those that a mesh axis runs over, the one named last changes fastest.
Arguments:
- saved_inputs: bfloat16 [2688, 4096], P('fs', 'tp'), may hold values from -6 to 6
- proj_cotangent: bfloat16 [2688, 4096], P('fs', 'tp'), may hold values from -0.115722656 to 0.115722656
- saved_hidden: bfloat16 [2688, 4096], P('fs', 'tp'), may hold values from -6 to 6
- out_cotangent: bfloat16 [2688, 4096], P('fs', 'tp'), may hold values from -0.115722656 to 0.115722656
- factors: bfloat16 [2, 4096, 128], replicated, may hold values from -0.46875 to 0.46875
- w_proj: float32 [4096, 4096], P('fs', 'tp'), may hold values from -0.09375 to 0.09375
- w_out: float32 [4096, 4096], P('tp', 'fs'), may hold values from -0.09375 to 0.09375
- moment_first: float32 [2, 128, 4096], P(None, None, 'tp'), may hold values from -1.8 to 1.8
- moment_second: float32 [2, 128, 4096], P(None, None, 'tp'), may hold values from 0.05 to 1
Outputs:
- proj_next: float32 [4096, 4096], P('fs', 'tp')
- out_next: float32 [4096, 4096], P('tp', 'fs')
- proj_copy: bfloat16 [4096, 4096], P(None, 'tp')
- out_copy: bfloat16 [4096, 4096], P('tp')
- first_next: float32 [2, 128, 4096], P(None, None, 'tp')
- second_next: float32 [2, 128, 4096], P(None, None, 'tp')
All inputs are finite; a program needn't handle non-finite values.
Results may differ from a plain program's by a relative error of at most 0.001.
Values may be sent and summed in bfloat16 or wider, within the bound.
A program may use at most 64 MiB of HBM per device.

v0:
```python
import functools

import jax
import jax.numpy as jnp
from jax import lax
from jax.experimental import pallas as pl
from jax.experimental.pallas import tpu as pltpu
from jax.sharding import PartitionSpec as P

beta_first = 0.9
beta_second = 0.95
learn_rate = 0.02
epsilon = 1e-06
weight_gain = 2500.0
code_top = 200.0
chunks = 4
MIB = 1024 * 1024
MESH = pl.DeviceIdType.MESH


def encode(x, gain, doublings):
    t = x * gain
    for _ in range(doublings):
        t = t * t
    return jnp.where(x < 0, -t, t).astype(jnp.bfloat16)


def decode(code, gain, doublings):
    v = code.astype(jnp.float32)
    size = jnp.exp2(jnp.log2(jnp.abs(v)) * (0.5**doublings)) * (1.0 / gain)
    return jnp.where(v < 0, -size, size)


def largest(x):
    top = jnp.max(jnp.max(jnp.abs(x), axis=0, keepdims=True), axis=1, keepdims=True)
    return jnp.maximum(top, 1e-30)


def two_parts(x, axis):
    high = x.astype(jnp.bfloat16)
    low = (x - high.astype(jnp.float32)).astype(jnp.bfloat16)
    return jnp.concatenate([high, low], axis=axis)


def proj_step(f, d0):
    return jnp.dot(jnp.concatenate([f, f], axis=1), d0[...], preferred_element_type=jnp.float32)


def out_step(f, d1):
    return lax.dot_general(
        d1[...],
        jnp.concatenate([f, f], axis=1),
        (((1,), (1,)), ((), ())),
        preferred_element_type=jnp.float32,
    )


def exchange_kernel(
    tp_count,
    entries,
    si_hbm,
    pc_hbm,
    sh_hbm,
    oc_hbm,
    f_hbm,
    wp_hbm,
    wo_hbm,
    mf_hbm,
    ms_hbm,
    first_ref,
    second_ref,
    d0_ref,
    d1_ref,
    gp_ref,
    go_ref,
    pn_ref,
    on_ref,
    fp_ref,
    fo_ref,
    si_ref,
    pc_ref,
    sh_ref,
    oc_ref,
    f_ref,
    wp_ref,
    wo_ref,
    mf_ref,
    ms_ref,
    cp,
    co,
    rows,
    rows_in,
    rows_all,
    part,
    part_code,
    part_in,
    grads,
    sq,
    sq_in,
    top_out,
    top_in,
    top_all,
    in_s,
    bulk_s,
    bulk_r,
    zs_s,
    zs_r,
    zg_s,
    zg_r,
    fs_s,
    fs_r,
    fg_s,
    fg_r,
    n_s,
    n_r,
    ts_s,
    ts_r,
    tg_s,
    tg_r,
):
    fs = lax.axis_index("fs")
    tp = lax.axis_index("tp")
    across_x = fs + 1 - 2 * lax.rem(fs, 2)
    across_y = lax.rem(fs + 2, 4)
    fs_peers = (across_x, across_y, 3 - fs)
    tp_peers = [lax.rem(tp + o, tp_count) for o in range(1, tp_count)]

    def send(src, dst, s_sem, r_sem, where):
        copy = pltpu.make_async_remote_copy(
            src_ref=src, dst_ref=dst, send_sem=s_sem, recv_sem=r_sem, device_id=where, device_id_type=MESH
        )
        copy.start()
        return copy

    barrier = pltpu.get_barrier_semaphore()
    for p in fs_peers:
        pl.semaphore_signal(barrier, inc=1, device_id={"fs": p}, device_id_type=MESH)
    for p in tp_peers:
        pl.semaphore_signal(barrier, inc=1, device_id={"tp": p}, device_id_type=MESH)
    pairs = (
        (wp_hbm, wp_ref),
        (wo_hbm, wo_ref),
        (f_hbm, f_ref),
        (si_hbm, si_ref),
        (oc_hbm, oc_ref),
        (pc_hbm, pc_ref),
        (sh_hbm, sh_ref),
        (mf_hbm, mf_ref),
        (ms_hbm, ms_ref),
    )
    loads = [pltpu.make_async_copy(a, b, in_s.at[i]) for i, (a, b) in enumerate(pairs)]
    for c in loads:
        c.start()
    loads[0].wait()
    cp[...] = encode(wp_ref[...], weight_gain, 4)
    pl.semaphore_wait(barrier, 3 + len(tp_peers))
    bulk = [send(cp, gp_ref.at[0], bulk_s.at[0], bulk_r.at[0], {"fs": across_x})]
    loads[1].wait()
    co[...] = encode(wo_ref[...], weight_gain, 4)
    bulk += [
        send(co, go_ref.at[1], bulk_s.at[1], bulk_r.at[1], {"fs": across_y}),
        send(co, go_ref.at[0], bulk_s.at[2], bulk_r.at[2], {"fs": across_x}),
        send(cp, gp_ref.at[1], bulk_s.at[3], bulk_r.at[3], {"fs": across_y}),
    ]
    for c in loads[2:5]:
        c.wait()

    tokens, feats = si_ref.shape
    own = pl.ds(pl.multiple_of(tp * feats, feats), feats)
    rows[:tokens, :] = jnp.dot(si_ref[...], f_ref[0, own, :], preferred_element_type=jnp.float32)
    rows[tokens:, :] = jnp.dot(oc_ref[...], f_ref[1, own, :], preferred_element_type=jnp.float32)
    piece = rows_in.shape[1]

    def rows_of(i):
        return pl.ds(pl.multiple_of(i * piece, 8), piece)

    copies = [
        send(rows.at[rows_of(p), :], rows_in.at[i], zs_s.at[i], zs_r.at[i], {"tp": p})
        for i, p in enumerate(tp_peers)
    ]
    for c in copies:
        c.wait_recv()
    total = rows[rows_of(tp), :]
    for i in range(tp_count - 1):
        total = total + rows_in[i]
    rows_all[rows_of(tp), :] = total
    gathers = [
        send(rows_all.at[rows_of(tp), :], rows_all.at[rows_of(tp), :], zg_s.at[i], zg_r.at[i], {"tp": p})
        for i, p in enumerate(tp_peers)
    ]
    for c in copies:
        c.wait_send()
    for c in loads[5:]:
        c.wait()
    for c in gathers:
        c.wait_recv()

    rank = f_ref.shape[2]
    slab = part_in.shape[1]
    for k, right in enumerate((pc_ref, sh_ref)):
        left = two_parts(rows_all[k * tokens : (k + 1) * tokens, :], 1)
        both = lax.dot_general(
            left, right[...], (((0,), (0,)), ((), ())), preferred_element_type=jnp.float32
        )
        both = both[:rank] + both[rank:]
        part[k * rank : (k + 1) * rank, :] = both
        for h in range(rank // slab):
            mine = both[h * slab : (h + 1) * slab]
            top = largest(mine)
            start = k * rank + h * slab
            top_out[start // slab] = jnp.broadcast_to(top, sq.shape)
            part_code[start : start + slab, :] = encode(mine, code_top / top, 4)
    for c in gathers:
        c.wait_send()

    def slab_of(i):
        return pl.ds(pl.multiple_of(i * slab, slab), slab)

    copies = [
        send(part_code.at[slab_of(p), :], part_in.at[i], fs_s.at[i], fs_r.at[i], {"fs": p})
        for i, p in enumerate(fs_peers)
    ]
    copies += [
        send(top_out.at[p], top_in.at[i], ts_s.at[i], ts_r.at[i], {"fs": p}) for i, p in enumerate(fs_peers)
    ]
    d_rows, width = cp.shape

    def relay(start, stop, at):
        a = pl.ds(start * d_rows // 8, (stop - start) * d_rows // 8)
        b = pl.ds(start * width // 8, (stop - start) * width // 8)
        return [
            send(gp_ref.at[0, a, :], gp_ref.at[2, a, :], bulk_s.at[at], bulk_r.at[at], {"fs": across_y}),
            send(
                go_ref.at[1, b, :], go_ref.at[2, b, :], bulk_s.at[at + 1], bulk_r.at[at + 1], {"fs": across_x}
            ),
        ]

    bulk[0].wait_recv()
    bulk[1].wait_recv()
    bulk += relay(0, 1, 4)
    for c in copies:
        c.wait_recv()
    total = part[slab_of(fs), :]
    for i in range(3):
        total = total + decode(part_in[i], code_top / top_in[i][0:1, 0:1], 4)
    top = largest(total)
    top_all[fs] = jnp.broadcast_to(top, sq.shape)
    grads[slab_of(fs), :] = encode(total, code_top / top, 4)
    gathers = [
        send(grads.at[slab_of(fs), :], grads.at[slab_of(fs), :], fg_s.at[i], fg_r.at[i], {"fs": p})
        for i, p in enumerate(fs_peers)
    ]
    gathers += [
        send(top_all.at[fs], top_all.at[fs], tg_s.at[i], tg_r.at[i], {"fs": p}) for i, p in enumerate(fs_peers)
    ]
    bulk += relay(1, 8, 6)
    for c in copies:
        c.wait_send()
    for c in gathers:
        c.wait_recv()
    small = jnp.concatenate(
        [
            decode(grads[j * slab : (j + 1) * slab, :], code_top / top_all[j][0:1, 0:1], 4)
            for j in range(2 * rank // slab)
        ],
        axis=0,
    )
    first = beta_first * mf_ref[...] + (1.0 - beta_first) * small
    second = beta_second * ms_ref[...] + (1.0 - beta_second) * small * small
    first_ref[...] = first
    second_ref[...] = second
    direction = first / (jnp.sqrt(second) + epsilon)
    for c in gathers:
        c.wait_send()

    d_model = f_ref.shape[1]
    step = d_model // 8
    squares = []
    for k in range(2):
        thin = two_parts(direction[k * rank : (k + 1) * rank], 0)

        def add(i, acc, k=k, thin=thin):
            f = f_ref[k, pl.ds(pl.multiple_of(i * step, step), step), :]
            u = jnp.dot(jnp.concatenate([f, f], axis=1), thin, preferred_element_type=jnp.float32)
            return acc + jnp.sum(u * u, axis=0, keepdims=True)

        acc = lax.fori_loop(0, 8, add, jnp.zeros((1, width), jnp.float32))
        squares.append(jnp.sum(acc, axis=1, keepdims=True))
    row = lax.broadcasted_iota(jnp.int32, sq.shape, 0)
    sq[...] = jnp.where(row == 0, squares[0], squares[1])
    norms = [send(sq, sq_in.at[i], n_s.at[i], n_r.at[i], {"tp": p}) for i, p in enumerate(tp_peers)]
    for c in norms:
        c.wait_recv()
    total = sq[...]
    for i in range(tp_count - 1):
        total = total + sq_in[i]
    scale = -learn_rate * lax.rsqrt(total / entries + epsilon)
    d0_ref[...] = two_parts(direction[:rank] * scale[0:1, 0:1], 0)
    d1_ref[...] = two_parts(jnp.transpose(direction[rank:] * scale[1:2, 0:1]), 1)
    for c in norms:
        c.wait_send()

    size = d_rows // chunks

    def block(slot, owner, proj_code, out_code):
        def one(i, _):
            at = pl.ds(pl.multiple_of(i * size, size), size)
            there = pl.ds(pl.multiple_of(owner * d_rows + i * size, size), size)
            u = proj_step(f_ref[0, there, :], d0_ref)
            fp_ref[slot, at, :] = (decode(proj_code[at, :], weight_gain, 4) + u).astype(jnp.bfloat16)
            if slot == 0:
                pn_ref[at, :] = wp_ref[at, :] + u
            u = out_step(f_ref[1, there, :], d1_ref)
            fo_ref[slot, :, at] = (decode(out_code[:, at], weight_gain, 4) + u).astype(jnp.bfloat16)
            if slot == 0:
                on_ref[:, at] = wo_ref[:, at] + u
            return 0

        lax.fori_loop(0, chunks, one, 0)

    block(0, fs, cp, co)
    bulk[2].wait_recv()
    block(1, across_x, gp_ref.at[0], go_ref.at[0])
    bulk[3].wait_recv()
    block(2, across_y, gp_ref.at[1], go_ref.at[1])
    for c in bulk[4:]:
        c.wait_recv()
    for c in bulk:
        c.wait_send()


def finish_kernel(
    me_ref, f_ref, d0, d1, gp, go, pn, on, fp, fo, mf, ms,
    pn_hbm, on_hbm, pc_hbm, oc_hbm, first_hbm, second_hbm, last_p, last_o, sems
):
    me = me_ref[0]
    d_rows = pn.shape[0]
    size = d_rows // chunks

    def span(owner, i=0, n=d_rows):
        return pl.ds(pl.multiple_of(owner * d_rows + i * n, n), n)

    owners = (me, me ^ 1, me ^ 2)
    pairs = [(pn, pn_hbm), (on, on_hbm), (mf, first_hbm), (ms, second_hbm)]
    for r, owner in enumerate(owners):
        pairs += [(fp.at[r], pc_hbm.at[span(owner), :]), (fo.at[r], oc_hbm.at[:, span(owner)])]
    copies = [pltpu.make_async_copy(a, b, sems.at[i]) for i, (a, b) in enumerate(pairs)]
    for c in copies:
        c.start()
    for i in range(chunks):
        at = pl.ds(i * size, size)
        there = span(me ^ 3, i, size)
        u = proj_step(f_ref[0, there, :], d0)
        last_p[at, :] = (decode(gp[2, at, :], weight_gain, 4) + u).astype(jnp.bfloat16)
        u = out_step(f_ref[1, there, :], d1)
        last_o[:, at] = (decode(go[2, :, at], weight_gain, 4) + u).astype(jnp.bfloat16)
        for a, b in ((last_p.at[at, :], pc_hbm.at[there, :]), (last_o.at[:, at], oc_hbm.at[:, there])):
            c = pltpu.make_async_copy(a, b, sems.at[len(copies)])
            c.start()
            copies.append(c)
    for c in copies:
        c.wait()


def fast_body(si, pc, sh, oc, factors, w_proj, w_out, m1, m2):
    fs_count, tp_count = lax.axis_size("fs"), lax.axis_size("tp")
    kinds, d_model, rank = factors.shape
    tokens = si.shape[0]
    width = pc.shape[1]
    d_rows = w_proj.shape[0]
    f32, bf16 = jnp.float32, jnp.bfloat16
    mf, ms = m1.reshape(2 * rank, width), m2.reshape(2 * rank, width)
    vm = pl.BlockSpec(memory_space=pltpu.VMEM)
    hbm = pl.BlockSpec(memory_space=pltpu.HBM)
    dma = lambda n: pltpu.SemaphoreType.DMA((n,))
    shape = jax.ShapeDtypeStruct
    peers = tp_count - 1
    piece = 2 * tokens // tp_count
    slab = 2 * rank // fs_count
    args = (si, pc, sh, oc, factors, w_proj, w_out, mf, ms)
    held = tuple(pltpu.with_memory_space_constraint(a, pltpu.HBM) for a in args)
    first, second, d0, d1, gp, go, pn, on, fp, fo = pl.pallas_call(
        functools.partial(exchange_kernel, tp_count, float(d_model * width * tp_count)),
        out_shape=(
            pltpu.VMEM((2 * rank, width), f32),
            pltpu.VMEM((2 * rank, width), f32),
            pltpu.VMEM((2 * rank, width), bf16),
            pltpu.VMEM((width, 2 * rank), bf16),
            pltpu.VMEM((3, d_rows, width), bf16),
            pltpu.VMEM((3, width, d_rows), bf16),
            pltpu.VMEM((d_rows, width), f32),
            pltpu.VMEM((width, d_rows), f32),
            pltpu.VMEM((3, d_rows, width), bf16),
            pltpu.VMEM((3, width, d_rows), bf16),
        ),
        in_specs=[hbm] * 9,
        out_specs=(vm,) * 10,
        scratch_shapes=[pltpu.VMEM(a.shape, a.dtype) for a in args]
        + [
            pltpu.VMEM((d_rows, width), bf16),
            pltpu.VMEM((width, d_rows), bf16),
            pltpu.VMEM((2 * tokens, rank), f32),
            pltpu.VMEM((peers, piece, rank), f32),
            pltpu.VMEM((2 * tokens, rank), f32),
            pltpu.VMEM((2 * rank, width), f32),
            pltpu.VMEM((2 * rank, width), bf16),
            pltpu.VMEM((3, slab, width), bf16),
            pltpu.VMEM((2 * rank, width), bf16),
            pltpu.VMEM((8, 128), f32),
            pltpu.VMEM((peers, 8, 128), f32),
            pltpu.VMEM((fs_count, 8, 128), f32),
            pltpu.VMEM((3, 8, 128), f32),
            pltpu.VMEM((fs_count, 8, 128), f32),
            dma(9),
            dma(8),
            dma(8),
            dma(peers),
            dma(peers),
            dma(peers),
            dma(peers),
            dma(3),
            dma(3),
            dma(3),
            dma(3),
            dma(peers),
            dma(peers),
            dma(3),
            dma(3),
            dma(3),
            dma(3),
        ],
        compiler_params=pltpu.CompilerParams(
            collective_id=0, has_side_effects=True, vmem_limit_bytes=40 * MIB
        ),
        name="exchange",
    )(*held)

    me = lax.axis_index("fs").astype(jnp.int32).reshape(1)
    pn, on, pcopy, ocopy, first, second = pl.pallas_call(
        finish_kernel,
        in_specs=[pl.BlockSpec(memory_space=pltpu.SMEM)] + [vm] * 11,
        out_specs=[hbm] * 6,
        out_shape=(
            shape(w_proj.shape, f32),
            shape(w_out.shape, f32),
            shape((d_model, width), bf16),
            shape((width, d_model), bf16),
            shape((2 * rank, width), f32),
            shape((2 * rank, width), f32),
        ),
        scratch_shapes=[
            pltpu.VMEM((d_rows, width), bf16),
            pltpu.VMEM((width, d_rows), bf16),
            dma(10 + 2 * chunks),
        ],
        compiler_params=pltpu.CompilerParams(vmem_limit_bytes=14 * MIB),
        name="finish",
    )(me, factors, d0, d1, gp, go, pn, on, fp, fo, first, second)
    return pn, on, pcopy, ocopy, first.reshape(m1.shape), second.reshape(m2.shape)


def over_tokens(left_rows, right_rows, precise):
    return lax.dot_general(
        left_rows,
        right_rows,
        (((0,), (0,)), ((), ())),
        preferred_element_type=jnp.float32,
        precision=precise,
    )


def body(
    saved_inputs,
    proj_cotangent,
    saved_hidden,
    out_cotangent,
    factors,
    w_proj,
    w_out,
    moment_first,
    moment_second,
):
    highest = lax.Precision.HIGHEST
    fs_count = lax.axis_size("fs")
    tp_count = lax.axis_size("tp")
    d_model = factors.shape[1]
    hidden_width = proj_cotangent.shape[1]
    fs_rows = d_model // fs_count
    tp_feats = saved_inputs.shape[1]
    own_rows = lax.dynamic_slice_in_dim(factors, lax.axis_index("fs") * fs_rows, fs_rows, 1).astype(
        jnp.float32
    )
    own_feats = lax.dynamic_slice_in_dim(factors, lax.axis_index("tp") * tp_feats, tp_feats, 1)
    proj_rows = jnp.dot(saved_inputs, own_feats[0], preferred_element_type=jnp.float32)
    out_rows = jnp.dot(out_cotangent, own_feats[1], preferred_element_type=jnp.float32)
    proj_rows, out_rows = lax.psum((proj_rows, out_rows), "tp")
    partial_sums = jnp.stack(
        [
            over_tokens(proj_rows, proj_cotangent.astype(jnp.float32), highest),
            over_tokens(out_rows, saved_hidden.astype(jnp.float32), highest),
        ]
    )
    small_grads = lax.psum(partial_sums, "fs")
    first_next = beta_first * moment_first + (1.0 - beta_first) * small_grads
    second_next = beta_second * moment_second + (1.0 - beta_second) * small_grads * small_grads
    direction = first_next / (jnp.sqrt(second_next) + epsilon)
    update_full = jnp.einsum("kdr,kre->kde", own_rows, direction, precision=highest)
    squares = lax.psum(jnp.sum(update_full * update_full, axis=(1, 2)), ("fs", "tp"))
    norm_scale = lax.rsqrt(squares / (d_model * hidden_width * tp_count) + epsilon)
    stepped = update_full * norm_scale[:, None, None]
    proj_next = w_proj - learn_rate * stepped[0]
    out_next = w_out - learn_rate * stepped[1].T
    proj_copy, out_copy = (
        lax.all_gather(proj_next.astype(jnp.bfloat16), "fs", axis=0, tiled=True),
        lax.all_gather(out_next.astype(jnp.bfloat16), "fs", axis=1, tiled=True),
    )
    return (proj_next, out_next, proj_copy, out_copy, first_next, second_next)


def solution(mesh):
    placed = (
        P("fs", "tp"),
        P("fs", "tp"),
        P("fs", "tp"),
        P("fs", "tp"),
        P(),
        P("fs", "tp"),
        P("tp", "fs"),
        P(None, None, "tp"),
        P(None, None, "tp"),
    )
    planned = fast_body if mesh.shape["fs"] == 4 and mesh.shape["tp"] == 8 else body
    return jax.shard_map(
        planned,
        mesh=mesh,
        in_specs=placed,
        out_specs=(
            P("fs", "tp"),
            P("tp", "fs"),
            P(None, "tp"),
            P("tp", None),
            P(None, None, "tp"),
            P(None, None, "tp"),
        ),
        check_vma=False,
    )
```

profile of v0, /device:TPU:1, one launch (start us, length us, event | category | flops | bytes accessed | tf_op | source)
XLA Modules:
  0.0 87.2 jit_solution(13036973224415180728)
XLA Ops:
  0.6 0.0 copy-start
  0.6 81.5 %exchange.1 = (f32[256,512]{1,0:T(8,128)S(1)}, f32[256,512]{1,0:T(8,128)S(1)}, bf16[256,512]{1,0:T(8,128)(2,1)S(1)}, bf16[512,256]{1,0:T(8,128)(2,1)S(1)}, bf16[...) custom-call(bf16[672,512]{1,0:T(8,128)(2,1)} %si_hbm.1, ...), custom_call_target="tpu_custom_call" | custom-call | tf_op jit(solution)/shard_map/exchange/pallas_call | solution.py:382
  82.1 0.0 copy-done
  82.2 5.0 %finish.1 = (f32[1024,512]{1,0:T(8,128)}, f32[512,1024]{1,0:T(8,128)}, bf16[4096,512]{1,0:T(8,128)(2,1)}, bf16[512,4096]{1,0:T(8,128)(2,1)}, f32[256,512]{1,0:T(8,128)}, /*index=5*/f32[256,512]{1,0:T(8,128)}) custom-call(s32[1]{0:T(128)} %bitcast.me_ref, bf16[2,4096,128]{2,1,0:T(8,128)(2,1)S(1)} %copy-done, bf16[256,512]{1,0:T(8,128)(2,1)S(1)} %get-tuple-element.22.d0, ...), custom_call_target="tpu_custom_call" | custom-call | tf_op jit(solution)/shard_map/finish/pallas_call | solution.py:439
Async XLA Ops:
  0.6 81.5 %copy-start = (bf16[2,4096,128]{2,1,0:T(8,128)(2,1)S(1)}, bf16[2,4096,128]{2,1,0:T(8,128)(2,1)}, u32[]{:S(2)}) copy-start(bf16[2,4096,128]{2,1,0:T(8,128)(2,1)} %f_ref.1) | copy-start | bytes 6291460
where the time goes:
time: 88.3 us; the launch traced here: 87.2 us
  Pallas kernels  86.5 us (98%)
    pallas_call x1, Pallas kernels, fast_body(): pl.pallas_call(functools.partial(exchange_kernel, tp_count, float(d_model...  81.5 us
    pallas_call x1, Pallas kernels, fast_body(): pl.pallas_call(finish_kernel, in_specs=[pl.BlockSpec(memory_space=pltpu.S...  5.02 us

commit v1 on v0

v1 whole, which is shorter than its diff:
```python
import functools

import jax
import jax.numpy as jnp
from jax import lax
from jax.experimental import pallas as pl
from jax.experimental.pallas import tpu as pltpu
from jax.sharding import PartitionSpec as P

beta_first = 0.9
beta_second = 0.95
learn_rate = 0.02
epsilon = 1e-06
weight_gain = 2500.0
code_top = 200.0
chunks = 4
pieces = 16
pad_rows = 16
MIB = 1024 * 1024
MESH = pl.DeviceIdType.MESH


def encode(x, gain, doublings):
    t = x * gain
    for _ in range(doublings):
        t = t * t
    return jnp.where(x < 0, -t, t).astype(jnp.bfloat16)


def decode(code, gain, doublings):
    v = code.astype(jnp.float32)
    size = jnp.exp2(jnp.log2(jnp.abs(v)) * (0.5**doublings)) * (1.0 / gain)
    return jnp.where(v < 0, -size, size)


def largest(x):
    top = jnp.max(jnp.max(jnp.abs(x), axis=0, keepdims=True), axis=1, keepdims=True)
    return jnp.maximum(top, 1e-30)


def two_parts(x, axis):
    high = x.astype(jnp.bfloat16)
    low = (x - high.astype(jnp.float32)).astype(jnp.bfloat16)
    return jnp.concatenate([high, low], axis=axis)


def proj_step(f, d0):
    return jnp.dot(jnp.concatenate([f, f], axis=1), d0[...], preferred_element_type=jnp.float32)


def out_step(f, d1):
    return lax.dot_general(
        d1[...],
        jnp.concatenate([f, f], axis=1),
        (((1,), (1,)), ((), ())),
        preferred_element_type=jnp.float32,
    )


def pack(ref, x):
    top = largest(x).astype(jnp.bfloat16)
    ref[: x.shape[0], :] = encode(x, code_top / top.astype(jnp.float32), 4)
    ref[ref.shape[0] - pad_rows :, :] = jnp.broadcast_to(top, (pad_rows, x.shape[1]))


def unpack(ref, n):
    top = ref[ref.shape[0] - pad_rows :, :][0:1, 0:1].astype(jnp.float32)
    return decode(ref[:n, :], code_top / top, 4)


def exchange_kernel(
    tp_count,
    entries,
    si_hbm,
    pc_hbm,
    sh_hbm,
    oc_hbm,
    f_hbm,
    wp_hbm,
    wo_hbm,
    mf_hbm,
    ms_hbm,
    first_ref,
    second_ref,
    d0_ref,
    d1_ref,
    gp_ref,
    go_ref,
    pn_ref,
    on_ref,
    fp_ref,
    fo_ref,
    si_ref,
    pc_ref,
    sh_ref,
    oc_ref,
    f_ref,
    wp_ref,
    wo_ref,
    mf_ref,
    ms_ref,
    cp,
    co,
    rows,
    pair_in,
    half,
    zc,
    zin,
    zall,
    part,
    step_a,
    step_b,
    in_a,
    in_b,
    quarters,
    sq,
    sq_in,
    known,
    in_s,
    out_s,
    out_r,
):
    fs = lax.axis_index("fs")
    tp = lax.axis_index("tp")
    core = lax.rem(tp, 2)
    z = tp // 2
    z_count = tp_count // 2
    across_x = fs + 1 - 2 * lax.rem(fs, 2)
    across_y = lax.rem(fs + 2, 4)
    diagonal = 3 - fs
    partner = tp + 1 - 2 * core
    z_peers = [2 * lax.rem(z + o, z_count) + core for o in range(1, z_count)]
    tp_peers = [lax.rem(tp + o, tp_count) for o in range(1, tp_count)]
    to_x, to_y = {"fs": across_x}, {"fs": across_y}

    def send(src, dst, where, s, r):
        copy = pltpu.make_async_remote_copy(
            src_ref=src,
            dst_ref=dst,
            send_sem=out_s.at[s],
            recv_sem=out_r.at[r],
            device_id=where,
            device_id_type=MESH,
        )
        copy.start()
        return copy

    def whole(ref, s, r):
        return pltpu.make_async_remote_copy(
            src_ref=ref,
            dst_ref=ref,
            send_sem=out_s.at[s],
            recv_sem=out_r.at[r],
            device_id={"tp": partner},
            device_id_type=MESH,
        )

    def signal(sem, where):
        pl.semaphore_signal(sem, inc=1, device_id=where, device_id_type=MESH)

    barrier = pltpu.get_barrier_semaphore()

    @pl.when(core == 0)
    def _():
        signal(barrier, to_x)
        signal(barrier, to_y)

    @pl.when(core == 1)
    def _():
        signal(barrier, {"tp": partner})

    d_rows, width = cp.shape

    def share(n, start, stop, of=chunks):
        return pl.ds(start * n // of, (stop - start) * n // of)

    pairs = []
    for start, stop in ((0, 1), (1, chunks)):
        a, b = share(d_rows, start, stop), share(width, start, stop)
        pairs += [(wp_hbm.at[a, :], wp_ref.at[a, :]), (wo_hbm.at[b, :], wo_ref.at[b, :])]
    pairs += [
        (f_hbm, f_ref),
        (si_hbm, si_ref),
        (oc_hbm, oc_ref),
        (pc_hbm, pc_ref),
        (sh_hbm, sh_ref),
        (mf_hbm, mf_ref),
        (ms_hbm, ms_ref),
    ]
    loads = [pltpu.make_async_copy(a, b, in_s.at[i]) for i, (a, b) in enumerate(pairs)]
    for c in loads:
        c.start()

    loads[0].wait()
    cp[share(d_rows, 0, 1), :] = encode(wp_ref[share(d_rows, 0, 1), :], weight_gain, 4)

    @pl.when(core == 0)
    def _():
        pl.semaphore_wait(barrier, 3)
        signal(known.at[0], to_x)
        signal(known.at[0], to_y)

    @pl.when(core == 1)
    def _():
        pl.semaphore_wait(known.at[0], 1)
        for p in z_peers:
            signal(barrier, {"tp": p})

    for i in range(chunks):
        a, b = share(d_rows, i, i + 1), share(width, i, i + 1)
        if i == 1:
            loads[2].wait()
        if i:
            cp[a, :] = encode(wp_ref[a, :], weight_gain, 4)
        send(cp.at[a, :], gp_ref.at[0, a, :], to_x, 0, 0)
        if i < 2:
            loads[2 * i + 1].wait()
        co[b, :] = encode(wo_ref[b, :], weight_gain, 4)
        send(co.at[b, :], go_ref.at[1, b, :], to_y, 1, 1)
        if i == 0:

            @pl.when(core == 0)
            def _():
                pl.semaphore_wait(known.at[0], 2)
                signal(known.at[0], {"tp": partner})

    def more(start, stop):
        a, b = share(d_rows, start, stop, pieces), share(width, start, stop, pieces)
        send(co.at[b, :], go_ref.at[0, b, :], to_x, 0, 2)
        send(cp.at[a, :], gp_ref.at[1, a, :], to_y, 1, 3)

    cuts = (0, 2, 5, 8, 11, 16)
    more(cuts[0], cuts[1])
    for c in loads[4:7]:
        c.wait()

    tokens, feats = si_ref.shape
    own = pl.ds(pl.multiple_of(tp * feats, feats), feats)
    rows[0] = jnp.dot(si_ref[...], f_ref[0, own, :], preferred_element_type=jnp.float32)
    rows[1] = jnp.dot(oc_ref[...], f_ref[1, own, :], preferred_element_type=jnp.float32)
    paired = send(rows.at[1 - core], pair_in, {"tp": partner}, 2, 4)
    for c in loads[7:]:
        c.wait()
    rank = f_ref.shape[2]
    grams = [
        lax.dot_general(f_ref[k], f_ref[k], (((0,), (0,)), ((), ())), preferred_element_type=jnp.float32)
        for k in range(2)
    ]
    paired.wait_recv()
    half[...] = rows[core] + pair_in[...]
    piece = tokens // z_count

    def piece_of(i):
        return pl.ds(pl.multiple_of(i * piece, 8), piece)

    @pl.when(core == 1)
    def _():
        pl.semaphore_wait(barrier, z_count - 1)
        signal(known.at[1], {"tp": partner})

    @pl.when(core == 0)
    def _():
        pl.semaphore_wait(known.at[1], 1)

    scatter = []
    for i, p in enumerate(z_peers):
        pack(zc.at[i], half[piece_of(lax.rem(z + i + 1, z_count)), :])
        scatter.append(send(zc.at[i], zin.at[i], {"tp": p}, 3, 5 + i))
    total = half[piece_of(z), :]
    for i, c in enumerate(scatter):
        c.wait_recv()
        total = total + unpack(zin.at[i], piece)
    pack(zall.at[core, z], total)
    def hand(at, where, s, r):
        return send(zall.at[core, at], zall.at[core, at], where, s, r)

    gathers = [hand(z, {"tp": p}, 4, 8 + i) for i, p in enumerate(z_peers)]
    hand(z, {"tp": partner}, 5, 11)
    for i, c in enumerate(gathers):
        c.wait_recv()
        hand(lax.rem(z + z_count - 1 - i, z_count), {"tp": partner}, 5, 11)
    passed = whole(zall.at[core], 5, 11)
    passed.wait_recv()
    paired.wait_send()
    whole(zc, 3, 5).wait_send()
    whole(zc, 4, 5).wait_send()
    passed.wait_send()

    for k, right in enumerate((pc_ref, sh_ref)):
        for i in range(z_count):
            rows[k, i * piece : (i + 1) * piece, :] = unpack(zall.at[k, i], piece)
        left = two_parts(rows[k], 1)
        both = lax.dot_general(
            left, right[...], (((0,), (0,)), ((), ())), preferred_element_type=jnp.float32
        )
        both = both[:rank] + both[rank:]
        for j in range(4):
            part[k, j] = both[:, j * width // 4 : (j + 1) * width // 4]

    pack(step_a.at[0], part[0, across_x])
    pack(step_a.at[1], part[0, diagonal])
    pack(step_b.at[0], part[1, across_y])
    pack(step_b.at[1], part[1, diagonal])
    sums = [
        send(step_a.at[0:2], in_a.at[0:2], to_x, 3, 12),
        send(step_b.at[0:2], in_b.at[0:2], to_y, 4, 13),
    ]
    more(cuts[1], cuts[2])
    sums[0].wait_recv()
    pack(step_a.at[2], part[0, across_y] + unpack(in_a.at[1], rank))
    sums.append(send(step_a.at[2], in_a.at[2], to_y, 3, 14))
    sums[1].wait_recv()
    pack(step_b.at[2], part[1, across_x] + unpack(in_b.at[1], rank))
    sums.append(send(step_b.at[2], in_b.at[2], to_x, 4, 15))
    more(cuts[2], cuts[3])
    mine_a = part[0, fs] + unpack(in_a.at[0], rank)
    mine_b = part[1, fs] + unpack(in_b.at[0], rank)
    sums[2].wait_recv()
    pack(quarters.at[0, fs], mine_a + unpack(in_a.at[2], rank))

    def spread(k, at, where, r):
        return send(quarters.at[k, at], quarters.at[k, at], where, 5 + k, r)

    from_y = spread(0, fs, to_y, 16)
    spread(0, fs, to_x, 18)
    sums[3].wait_recv()
    pack(quarters.at[1, fs], mine_b + unpack(in_b.at[2], rank))
    from_x = spread(1, fs, to_x, 17)
    spread(1, fs, to_y, 18)
    more(cuts[3], cuts[4])
    from_y.wait_recv()
    spread(0, across_y, to_x, 18)
    from_x.wait_recv()
    spread(1, across_x, to_y, 18)
    more(cuts[4], cuts[5])
    whole(gp_ref.at[0], 0, 0).wait_recv()
    whole(go_ref.at[1], 1, 1).wait_recv()
    relays = []
    for i in range(chunks):
        a = share(d_rows, i, i + 1)
        relays += [
            send(gp_ref.at[0, a, :], gp_ref.at[2, a, :], to_y, 1, 20 + 2 * i),
            send(go_ref.at[1, :, a], go_ref.at[2, :, a], to_x, 0, 21 + 2 * i),
        ]
    whole(quarters.at[0], 5, 18).wait_recv()
    whole(step_a, 3, 12).wait_send()
    whole(step_b, 4, 13).wait_send()
    whole(step_a, 5, 12).wait_send()
    whole(step_b, 6, 13).wait_send()

    highest = lax.Precision.HIGHEST
    squares = []
    directions = []
    for k in range(2):
        small = jnp.concatenate([unpack(quarters.at[k, j], rank) for j in range(4)], axis=1)
        at = slice(k * rank, (k + 1) * rank)
        first = beta_first * mf_ref[at, :] + (1.0 - beta_first) * small
        second = beta_second * ms_ref[at, :] + (1.0 - beta_second) * small * small
        first_ref[at, :] = first
        second_ref[at, :] = second
        direction = first / (jnp.sqrt(second) + epsilon)
        directions.append(direction)
        seen = jnp.dot(grams[k], direction, preferred_element_type=jnp.float32, precision=highest)
        seen = jnp.sum(seen * direction, axis=0, keepdims=True)
        squares.append(jnp.sum(seen, axis=1, keepdims=True))
    row = lax.broadcasted_iota(jnp.int32, sq.shape, 0)
    sq[...] = jnp.where(row == 0, squares[0], squares[1])
    for i, p in enumerate(tp_peers):
        send(sq, sq_in.at[i], {"tp": p}, 2, 19)
    whole(sq_in, 2, 19).wait_recv()
    total = sq[...]
    for i in range(tp_count - 1):
        total = total + sq_in[i]
    scale = -learn_rate * lax.rsqrt(jnp.maximum(total, 0.0) / entries + epsilon)
    d0_ref[...] = two_parts(directions[0] * scale[0:1, 0:1], 0)
    d1_ref[...] = two_parts(jnp.transpose(directions[1] * scale[1:2, 0:1]), 1)
    whole(sq_in, 2, 19).wait_send()

    size = d_rows // chunks

    def block(slot, owner, proj_code, out_code, start=0, stop=chunks):
        def one(i, _):
            at = pl.ds(pl.multiple_of(i * size, size), size)
            there = pl.ds(pl.multiple_of(owner * d_rows + i * size, size), size)
            u = proj_step(f_ref[0, there, :], d0_ref)
            fp_ref[slot, at, :] = (decode(proj_code[at, :], weight_gain, 4) + u).astype(jnp.bfloat16)
            if slot == 0:
                pn_ref[at, :] = wp_ref[at, :] + u
            u = out_step(f_ref[1, there, :], d1_ref)
            fo_ref[slot, :, at] = (decode(out_code[:, at], weight_gain, 4) + u).astype(jnp.bfloat16)
            if slot == 0:
                on_ref[:, at] = wo_ref[:, at] + u
            return 0

        lax.fori_loop(start, stop, one, 0)

    block(0, fs, cp, co)
    whole(go_ref.at[0], 0, 2).wait_recv()
    block(1, across_x, gp_ref.at[0], go_ref.at[0])
    whole(gp_ref.at[1], 1, 3).wait_recv()
    block(2, across_y, gp_ref.at[1], go_ref.at[1])
    for i in range(chunks - 1):
        relays[2 * i].wait_recv()
        relays[2 * i + 1].wait_recv()
        block(3, diagonal, gp_ref.at[2], go_ref.at[2], i, i + 1)
    for c in relays[2 * chunks - 2 :]:
        c.wait_recv()
    whole(go_ref, 0, 0).wait_send()
    whole(gp_ref, 1, 1).wait_send()


def finish_kernel(
    me_ref, f_ref, d0, d1, gp, go, pn, on, fp, fo, mf, ms,
    pn_hbm, on_hbm, pc_hbm, oc_hbm, first_hbm, second_hbm, last_p, last_o, sems
):
    me = me_ref[0]
    d_rows = pn.shape[0]
    size = d_rows // chunks
    early = d_rows - size

    def span(owner, n=d_rows, start=0):
        return pl.ds(pl.multiple_of(owner * d_rows + start, size), n)

    pairs = [(pn, pn_hbm), (on, on_hbm), (mf, first_hbm), (ms, second_hbm)]
    for r, owner in enumerate((me, me ^ 1, me ^ 2)):
        pairs += [(fp.at[r], pc_hbm.at[span(owner), :]), (fo.at[r], oc_hbm.at[:, span(owner)])]
    pairs += [
        (fp.at[3, :early, :], pc_hbm.at[span(me ^ 3, early), :]),
        (fo.at[3, :, :early], oc_hbm.at[:, span(me ^ 3, early)]),
    ]
    copies = [pltpu.make_async_copy(a, b, sems.at[i]) for i, (a, b) in enumerate(pairs)]
    for c in copies:
        c.start()
    there = span(me ^ 3, size, early)
    u = proj_step(f_ref[0, there, :], d0)
    last_p[...] = (decode(gp[2, early:, :], weight_gain, 4) + u).astype(jnp.bfloat16)
    copies.append(pltpu.make_async_copy(last_p, pc_hbm.at[there, :], sems.at[len(copies)]))
    copies[-1].start()
    u = out_step(f_ref[1, there, :], d1)
    last_o[...] = (decode(go[2, :, early:], weight_gain, 4) + u).astype(jnp.bfloat16)
    copies.append(pltpu.make_async_copy(last_o, oc_hbm.at[:, there], sems.at[len(copies)]))
    copies[-1].start()
    for c in copies:
        c.wait()


def fast_body(si, pc, sh, oc, factors, w_proj, w_out, m1, m2):
    tp_count = lax.axis_size("tp")
    kinds, d_model, rank = factors.shape
    tokens = si.shape[0]
    width = pc.shape[1]
    d_rows = w_proj.shape[0]
    f32, bf16 = jnp.float32, jnp.bfloat16
    mf, ms = m1.reshape(2 * rank, width), m2.reshape(2 * rank, width)
    vm = pl.BlockSpec(memory_space=pltpu.VMEM)
    hbm = pl.BlockSpec(memory_space=pltpu.HBM)
    dma = lambda n: pltpu.SemaphoreType.DMA((n,))
    shape = jax.ShapeDtypeStruct
    peers = tp_count - 1
    z_count = tp_count // 2
    piece = tokens // z_count
    packed = -(-piece // pad_rows) * pad_rows + pad_rows
    quarter = width // 4
    args = (si, pc, sh, oc, factors, w_proj, w_out, mf, ms)
    held = tuple(pltpu.with_memory_space_constraint(a, pltpu.HBM) for a in args)
    first, second, d0, d1, gp, go, pn, on, fp, fo = pl.pallas_call(
        functools.partial(exchange_kernel, tp_count, float(d_model * width * tp_count)),
        out_shape=(
            pltpu.VMEM((2 * rank, width), f32),
            pltpu.VMEM((2 * rank, width), f32),
            pltpu.VMEM((2 * rank, width), bf16),
            pltpu.VMEM((width, 2 * rank), bf16),
            pltpu.VMEM((3, d_rows, width), bf16),
            pltpu.VMEM((3, width, d_rows), bf16),
            pltpu.VMEM((d_rows, width), f32),
            pltpu.VMEM((width, d_rows), f32),
            pltpu.VMEM((4, d_rows, width), bf16),
            pltpu.VMEM((4, width, d_rows), bf16),
        ),
        in_specs=[hbm] * 9,
        out_specs=(vm,) * 10,
        scratch_shapes=[pltpu.VMEM(a.shape, a.dtype) for a in args]
        + [
            pltpu.VMEM((d_rows, width), bf16),
            pltpu.VMEM((width, d_rows), bf16),
            pltpu.VMEM((2, tokens, rank), f32),
            pltpu.VMEM((tokens, rank), f32),
            pltpu.VMEM((tokens, rank), f32),
            pltpu.VMEM((z_count - 1, packed, rank), bf16),
            pltpu.VMEM((z_count - 1, packed, rank), bf16),
            pltpu.VMEM((2, z_count, packed, rank), bf16),
            pltpu.VMEM((2, 4, rank, quarter), f32),
            pltpu.VMEM((3, rank + pad_rows, quarter), bf16),
            pltpu.VMEM((3, rank + pad_rows, quarter), bf16),
            pltpu.VMEM((3, rank + pad_rows, quarter), bf16),
            pltpu.VMEM((3, rank + pad_rows, quarter), bf16),
            pltpu.VMEM((2, 4, rank + pad_rows, quarter), bf16),
            pltpu.VMEM((8, 128), f32),
            pltpu.VMEM((peers, 8, 128), f32),
            pltpu.SemaphoreType.REGULAR((2,)),
            dma(11),
            dma(7),
            dma(20 + 2 * chunks),
        ],
        compiler_params=pltpu.CompilerParams(
            collective_id=0, has_side_effects=True, vmem_limit_bytes=42 * MIB
        ),
        name="exchange",
    )(*held)

    me = lax.axis_index("fs").astype(jnp.int32).reshape(1)
    pn, on, pcopy, ocopy, first, second = pl.pallas_call(
        finish_kernel,
        in_specs=[pl.BlockSpec(memory_space=pltpu.SMEM)] + [vm] * 11,
        out_specs=[hbm] * 6,
        out_shape=(
            shape(w_proj.shape, f32),
            shape(w_out.shape, f32),
            shape((d_model, width), bf16),
            shape((width, d_model), bf16),
            shape((2 * rank, width), f32),
            shape((2 * rank, width), f32),
        ),
        scratch_shapes=[
            pltpu.VMEM((d_rows // chunks, width), bf16),
            pltpu.VMEM((width, d_rows // chunks), bf16),
            dma(14),
        ],
        compiler_params=pltpu.CompilerParams(vmem_limit_bytes=8 * MIB),
        name="finish",
    )(me, factors, d0, d1, gp, go, pn, on, fp, fo, first, second)
    return pn, on, pcopy, ocopy, first.reshape(m1.shape), second.reshape(m2.shape)


def over_tokens(left_rows, right_rows, precise):
    return lax.dot_general(
        left_rows,
        right_rows,
        (((0,), (0,)), ((), ())),
        preferred_element_type=jnp.float32,
        precision=precise,
    )


def body(
    saved_inputs,
    proj_cotangent,
    saved_hidden,
    out_cotangent,
    factors,
    w_proj,
    w_out,
    moment_first,
    moment_second,
):
    highest = lax.Precision.HIGHEST
    fs_count = lax.axis_size("fs")
    tp_count = lax.axis_size("tp")
    d_model = factors.shape[1]
    hidden_width = proj_cotangent.shape[1]
    fs_rows = d_model // fs_count
    tp_feats = saved_inputs.shape[1]
    own_rows = lax.dynamic_slice_in_dim(factors, lax.axis_index("fs") * fs_rows, fs_rows, 1).astype(
        jnp.float32
    )
    own_feats = lax.dynamic_slice_in_dim(factors, lax.axis_index("tp") * tp_feats, tp_feats, 1)
    proj_rows = jnp.dot(saved_inputs, own_feats[0], preferred_element_type=jnp.float32)
    out_rows = jnp.dot(out_cotangent, own_feats[1], preferred_element_type=jnp.float32)
    proj_rows, out_rows = lax.psum((proj_rows, out_rows), "tp")
    partial_sums = jnp.stack(
        [
            over_tokens(proj_rows, proj_cotangent.astype(jnp.float32), highest),
            over_tokens(out_rows, saved_hidden.astype(jnp.float32), highest),
        ]
    )
    small_grads = lax.psum(partial_sums, "fs")
    first_next = beta_first * moment_first + (1.0 - beta_first) * small_grads
    second_next = beta_second * moment_second + (1.0 - beta_second) * small_grads * small_grads
    direction = first_next / (jnp.sqrt(second_next) + epsilon)
    update_full = jnp.einsum("kdr,kre->kde", own_rows, direction, precision=highest)
    squares = lax.psum(jnp.sum(update_full * update_full, axis=(1, 2)), ("fs", "tp"))
    norm_scale = lax.rsqrt(squares / (d_model * hidden_width * tp_count) + epsilon)
    stepped = update_full * norm_scale[:, None, None]
    proj_next = w_proj - learn_rate * stepped[0]
    out_next = w_out - learn_rate * stepped[1].T
    proj_copy, out_copy = (
        lax.all_gather(proj_next.astype(jnp.bfloat16), "fs", axis=0, tiled=True),
        lax.all_gather(out_next.astype(jnp.bfloat16), "fs", axis=1, tiled=True),
    )
    return (proj_next, out_next, proj_copy, out_copy, first_next, second_next)


def solution(mesh):
    placed = (
        P("fs", "tp"),
        P("fs", "tp"),
        P("fs", "tp"),
        P("fs", "tp"),
        P(),
        P("fs", "tp"),
        P("tp", "fs"),
        P(None, None, "tp"),
        P(None, None, "tp"),
    )
    planned = fast_body if mesh.shape["fs"] == 4 and mesh.shape["tp"] == 8 else body
    return jax.shard_map(
        planned,
        mesh=mesh,
        in_specs=placed,
        out_specs=(
            P("fs", "tp"),
            P("tp", "fs"),
            P(None, "tp"),
            P("tp", None),
            P(None, None, "tp"),
            P(None, None, "tp"),
        ),
        check_vma=False,
    )
```

time: 88.3 us -> 83.9 us (0.950); the launches traced: 87.2 us -> 83.8 us
  Pallas kernels: 86.5 us -> 83.1 us
    pallas_call x1, Pallas kernels: 81.5 us -> 78.2 us  [fast_body(): pl.pallas_call(functools.partial(exchange_kernel, tp_count, float(d_model...]
where the time goes in v1:
time: 83.9 us; the launch traced here: 83.8 us
  Pallas kernels  83.1 us (99%)
    pallas_call x1, Pallas kernels, fast_body(): pl.pallas_call(functools.partial(exchange_kernel, tp_count, float(d_model...  78.2 us
    pallas_call x1, Pallas kernels, fast_body(): pl.pallas_call(finish_kernel, in_specs=[pl.BlockSpec(memory_space=pltpu.S...  4.97 us

profile of v1, /device:TPU:1, one launch (start us, length us, event | category | flops | bytes accessed | tf_op | source)
XLA Modules:
  0.0 83.8 jit_solution(13014011829225622334)
XLA Ops:
  0.6 0.0 copy-start
  0.6 78.2 %exchange.1 = (f32[256,512]{1,0:T(8,128)S(1)}, f32[256,512]{1,0:T(8,128)S(1)}, bf16[256,512]{1,0:T(8,128)(2,1)S(1)}, bf16[512,256]{1,0:T(8,128)(2,1)S(1)}, bf16[...) custom-call(bf16[672,512]{1,0:T(8,128)(2,1)} %si_hbm.1, ...), custom_call_target="tpu_custom_call" | custom-call | tf_op jit(solution)/shard_map/exchange/pallas_call | solution.py:466
  78.8 0.0 copy-done
  78.8 5.0 %finish.1 = (f32[1024,512]{1,0:T(8,128)}, f32[512,1024]{1,0:T(8,128)}, bf16[4096,512]{1,0:T(8,128)(2,1)}, bf16[512,4096]{1,0:T(8,128)(2,1)}, f32[256,512]{1,0:T(8,128)}, /*index=5*/f32[256,512]{1,0:T(8,128)}) custom-call(s32[1]{0:T(128)} %bitcast.me_ref, bf16[2,4096,128]{2,1,0:T(8,128)(2,1)S(1)} %copy-done, bf16[256,512]{1,0:T(8,128)(2,1)S(1)} %get-tuple-element.22.d0, ...), custom_call_target="tpu_custom_call" | custom-call | tf_op jit(solution)/shard_map/finish/pallas_call | solution.py:512
Async XLA Ops:
  0.6 78.2 %copy-start = (bf16[2,4096,128]{2,1,0:T(8,128)(2,1)S(1)}, bf16[2,4096,128]{2,1,0:T(8,128)(2,1)}, u32[]{:S(2)}) copy-start(bf16[2,4096,128]{2,1,0:T(8,128)(2,1)} %f_ref.1) | copy-start | bytes 6291460

commit v2 on v1

--- a/solution.py
+++ b/solution.py
@@ -11,9 +11,10 @@
 beta_second = 0.95
 learn_rate = 0.02
 epsilon = 1e-06
-weight_gain = 2500.0
+weight_rate = 1344.0
 code_top = 200.0
 chunks = 4
+early = 1
 pieces = 16
 pad_rows = 16
 MIB = 1024 * 1024
@@ -55,6 +56,14 @@
         (((1,), (1,)), ((), ())),
         preferred_element_type=jnp.float32,
     )
+
+
+def weight_code(x):
+    return jnp.exp2(x * weight_rate).astype(jnp.bfloat16)
+
+
+def weight_of(code):
+    return jnp.log2(code.astype(jnp.float32)) * (1.0 / weight_rate)
 
 
 def pack(ref, x):
@@ -90,11 +99,11 @@
     on_ref,
     fp_ref,
     fo_ref,
+    f_ref,
     si_ref,
     pc_ref,
     sh_ref,
     oc_ref,
-    f_ref,
     wp_ref,
     wo_ref,
     mf_ref,
@@ -174,9 +183,10 @@
     def share(n, start, stop, of=chunks):
         return pl.ds(start * n // of, (stop - start) * n // of)
 
+    spans = ((0, 2), (2, 6), (6, 10), (10, 15))
     pairs = []
-    for start, stop in ((0, 1), (1, chunks)):
-        a, b = share(d_rows, start, stop), share(width, start, stop)
+    for start, stop in (spans[0], (spans[0][1], pieces)):
+        a, b = share(d_rows, start, stop, pieces), share(width, start, stop, pieces)
         pairs += [(wp_hbm.at[a, :], wp_ref.at[a, :]), (wo_hbm.at[b, :], wo_ref.at[b, :])]
     pairs += [
         (f_hbm, f_ref),
@@ -188,11 +198,30 @@
         (ms_hbm, ms_ref),
     ]
     loads = [pltpu.make_async_copy(a, b, in_s.at[i]) for i, (a, b) in enumerate(pairs)]
-    for c in loads:
+    for c in loads[:4]:
         c.start()
 
+
+    def encode_proj(start, stop):
+        a = share(d_rows, start, stop, pieces)
+        cp[a, :] = weight_code(wp_ref[a, :])
+
+    def encode_out(start, stop):
+        b = share(width, start, stop, pieces)
+        co[b, :] = weight_code(wo_ref[b, :])
+
+    def open_proj(start, stop):
+        a = share(d_rows, start, stop, pieces)
+        send(cp.at[a, :], gp_ref.at[0, a, :], to_x, 0, 0)
+
+    def open_out(start, stop):
+        b = share(width, start, stop, pieces)
+        send(co.at[b, :], go_ref.at[1, b, :], to_y, 1, 1)
+
     loads[0].wait()
-    cp[share(d_rows, 0, 1), :] = encode(wp_ref[share(d_rows, 0, 1), :], weight_gain, 4)
+    encode_proj(*spans[0])
+    loads[1].wait()
+    encode_out(*spans[0])
 
     @pl.when(core == 0)
     def _():
@@ -206,31 +235,33 @@
         for p in z_peers:
             signal(barrier, {"tp": p})
 
-    for i in range(chunks):
-        a, b = share(d_rows, i, i + 1), share(width, i, i + 1)
-        if i == 1:
-            loads[2].wait()
-        if i:
-            cp[a, :] = encode(wp_ref[a, :], weight_gain, 4)
-        send(cp.at[a, :], gp_ref.at[0, a, :], to_x, 0, 0)
-        if i < 2:
-            loads[2 * i + 1].wait()
-        co[b, :] = encode(wo_ref[b, :], weight_gain, 4)
-        send(co.at[b, :], go_ref.at[1, b, :], to_y, 1, 1)
-        if i == 0:
-
-            @pl.when(core == 0)
-            def _():
-                pl.semaphore_wait(known.at[0], 2)
-                signal(known.at[0], {"tp": partner})
+    open_proj(*spans[0])
+    open_out(*spans[0])
+    for c in loads[4:]:
+        c.start()
+
+    @pl.when(core == 0)
+    def _():
+        pl.semaphore_wait(known.at[0], 2)
+        signal(known.at[0], {"tp": partner})
+
+    loads[2].wait()
+    loads[3].wait()
+    for start, stop in spans[1:]:
+        encode_proj(start, stop)
+        open_proj(start, stop)
+        encode_out(start, stop)
+        open_out(start, stop)
+    last = spans[-1][1]
+    encode_proj(last, pieces)
+    encode_out(last, pieces)
 
     def more(start, stop):
         a, b = share(d_rows, start, stop, pieces), share(width, start, stop, pieces)
         send(co.at[b, :], go_ref.at[0, b, :], to_x, 0, 2)
         send(cp.at[a, :], gp_ref.at[1, a, :], to_y, 1, 3)
 
-    cuts = (0, 2, 5, 8, 11, 16)
-    more(cuts[0], cuts[1])
+    cuts = (0, 1, 3, 5, 16)
     for c in loads[4:7]:
         c.wait()
 
@@ -305,14 +336,16 @@
         send(step_a.at[0:2], in_a.at[0:2], to_x, 3, 12),
         send(step_b.at[0:2], in_b.at[0:2], to_y, 4, 13),
     ]
-    more(cuts[1], cuts[2])
+    open_proj(last, pieces)
+    open_out(last, pieces)
+    more(cuts[0], cuts[1])
     sums[0].wait_recv()
     pack(step_a.at[2], part[0, across_y] + unpack(in_a.at[1], rank))
     sums.append(send(step_a.at[2], in_a.at[2], to_y, 3, 14))
     sums[1].wait_recv()
     pack(step_b.at[2], part[1, across_x] + unpack(in_b.at[1], rank))
     sums.append(send(step_b.at[2], in_b.at[2], to_x, 4, 15))
-    more(cuts[2], cuts[3])
+    more(cuts[1], cuts[2])
     mine_a = part[0, fs] + unpack(in_a.at[0], rank)
     mine_b = part[1, fs] + unpack(in_b.at[0], rank)
     sums[2].wait_recv()
@@ -327,21 +360,28 @@
     pack(quarters.at[1, fs], mine_b + unpack(in_b.at[2], rank))
     from_x = spread(1, fs, to_x, 17)
     spread(1, fs, to_y, 18)
-    more(cuts[3], cuts[4])
+    more(cuts[2], cuts[3])
     from_y.wait_recv()
     spread(0, across_y, to_x, 18)
     from_x.wait_recv()
     spread(1, across_x, to_y, 18)
-    more(cuts[4], cuts[5])
+    more(cuts[3], cuts[4])
     whole(gp_ref.at[0], 0, 0).wait_recv()
     whole(go_ref.at[1], 1, 1).wait_recv()
-    relays = []
-    for i in range(chunks):
+
+    def relay(i):
         a = share(d_rows, i, i + 1)
-        relays += [
-            send(gp_ref.at[0, a, :], gp_ref.at[2, a, :], to_y, 1, 20 + 2 * i),
-            send(go_ref.at[1, :, a], go_ref.at[2, :, a], to_x, 0, 21 + 2 * i),
-        ]
+        send(gp_ref.at[0, a, :], gp_ref.at[2, a, :], to_y, 1, 20 + 2 * i)
+        send(go_ref.at[1, :, a], go_ref.at[2, :, a], to_x, 0, 21 + 2 * i)
+
+    for i in range(early):
+        relay(i)
+
+    @pl.when(core == 1)
+    def _():
+        for i in range(early, chunks):
+            relay(i)
+
     whole(quarters.at[0], 5, 18).wait_recv()
     whole(step_a, 3, 12).wait_send()
     whole(step_b, 4, 13).wait_send()
@@ -383,11 +423,11 @@
             at = pl.ds(pl.multiple_of(i * size, size), size)
             there = pl.ds(pl.multiple_of(owner * d_rows + i * size, size), size)
             u = proj_step(f_ref[0, there, :], d0_ref)
-            fp_ref[slot, at, :] = (decode(proj_code[at, :], weight_gain, 4) + u).astype(jnp.bfloat16)
+            fp_ref[slot, at, :] = (weight_of(proj_code[at, :]) + u).astype(jnp.bfloat16)
             if slot == 0:
                 pn_ref[at, :] = wp_ref[at, :] + u
             u = out_step(f_ref[1, there, :], d1_ref)
-            fo_ref[slot, :, at] = (decode(out_code[:, at], weight_gain, 4) + u).astype(jnp.bfloat16)
+            fo_ref[slot, :, at] = (weight_of(out_code[:, at]) + u).astype(jnp.bfloat16)
             if slot == 0:
                 on_ref[:, at] = wo_ref[:, at] + u
             return 0
@@ -399,49 +439,146 @@
     block(1, across_x, gp_ref.at[0], go_ref.at[0])
     whole(gp_ref.at[1], 1, 3).wait_recv()
     block(2, across_y, gp_ref.at[1], go_ref.at[1])
-    for i in range(chunks - 1):
-        relays[2 * i].wait_recv()
-        relays[2 * i + 1].wait_recv()
+
+    def relayed(i):
+        a = share(d_rows, i, i + 1)
+        whole(gp_ref.at[2, a, :], 1, 20 + 2 * i).wait_recv()
+        whole(go_ref.at[2, :, a], 0, 21 + 2 * i).wait_recv()
         block(3, diagonal, gp_ref.at[2], go_ref.at[2], i, i + 1)
-    for c in relays[2 * chunks - 2 :]:
-        c.wait_recv()
-    whole(go_ref, 0, 0).wait_send()
-    whole(gp_ref, 1, 1).wait_send()
-
-
-def finish_kernel(
-    me_ref, f_ref, d0, d1, gp, go, pn, on, fp, fo, mf, ms,
-    pn_hbm, on_hbm, pc_hbm, oc_hbm, first_hbm, second_hbm, last_p, last_o, sems
+
+    for i in range(early):
+        relayed(i)
+    whole(go_ref.at[0:2], 0, 0).wait_send()
+    whole(gp_ref.at[0:2], 1, 1).wait_send()
+    a = share(d_rows, 0, early)
+    whole(gp_ref.at[2, a, :], 1, 0).wait_send()
+    whole(go_ref.at[2, :, a], 0, 0).wait_send()
+
+    @pl.when(core == 1)
+    def _():
+        for i in range(early, chunks):
+            relayed(i)
+        a = share(d_rows, early, chunks)
+        whole(gp_ref.at[2, a, :], 1, 0).wait_send()
+        whole(go_ref.at[2, :, a], 0, 0).wait_send()
+
+
+def write_kernel(
+    me_ref, core_ref, pn, on, fp, fo, mf, ms,
+    pn_hbm, on_hbm, pc_hbm, oc_hbm, first_hbm, second_hbm, sems
 ):
     me = me_ref[0]
     d_rows = pn.shape[0]
     size = d_rows // chunks
-    early = d_rows - size
-
-    def span(owner, n=d_rows, start=0):
-        return pl.ds(pl.multiple_of(owner * d_rows + start, size), n)
+
+    def span(owner, start=0, stop=chunks):
+        return pl.ds(pl.multiple_of(owner * d_rows + start * size, size), (stop - start) * size)
+
+    def diagonal(start, stop):
+        a = pl.ds(start * size, (stop - start) * size)
+        there = span(me ^ 3, start, stop)
+        return [(fp.at[3, a, :], pc_hbm.at[there, :]), (fo.at[3, :, a], oc_hbm.at[:, there])]
 
     pairs = [(pn, pn_hbm), (on, on_hbm), (mf, first_hbm), (ms, second_hbm)]
     for r, owner in enumerate((me, me ^ 1, me ^ 2)):
         pairs += [(fp.at[r], pc_hbm.at[span(owner), :]), (fo.at[r], oc_hbm.at[:, span(owner)])]
-    pairs += [
-        (fp.at[3, :early, :], pc_hbm.at[span(me ^ 3, early), :]),
-        (fo.at[3, :, :early], oc_hbm.at[:, span(me ^ 3, early)]),
-    ]
+    pairs += diagonal(0, early)
     copies = [pltpu.make_async_copy(a, b, sems.at[i]) for i, (a, b) in enumerate(pairs)]
     for c in copies:
         c.start()
-    there = span(me ^ 3, size, early)
-    u = proj_step(f_ref[0, there, :], d0)
-    last_p[...] = (decode(gp[2, early:, :], weight_gain, 4) + u).astype(jnp.bfloat16)
-    copies.append(pltpu.make_async_copy(last_p, pc_hbm.at[there, :], sems.at[len(copies)]))
-    copies[-1].start()
-    u = out_step(f_ref[1, there, :], d1)
-    last_o[...] = (decode(go[2, :, early:], weight_gain, 4) + u).astype(jnp.bfloat16)
-    copies.append(pltpu.make_async_copy(last_o, oc_hbm.at[:, there], sems.at[len(copies)]))
-    copies[-1].start()
+
+    @pl.when(core_ref[0] == 1)
+    def _():
+        rest = [
+            pltpu.make_async_copy(a, b, sems.at[len(copies) + i])
+            for i, (a, b) in enumerate(diagonal(early, chunks))
+        ]
+        for c in rest:
+            c.start()
+        for c in rest:
+            c.wait()
+
     for c in copies:
         c.wait()
+
+
+def relay_kernel(f_ref, d0_ref, d1_ref, gp, go, lp_ref, lo_ref, fp_ref, fo_ref, out_s, out_r):
+    fs = lax.axis_index("fs")
+    core = lax.rem(lax.axis_index("tp"), 2)
+    to_x = {"fs": fs + 1 - 2 * lax.rem(fs, 2)}
+    to_y = {"fs": lax.rem(fs + 2, 4)}
+    d_rows = gp.shape[1]
+    size = d_rows // chunks
+
+    @pl.when(core == 0)
+    def _():
+        barrier = pltpu.get_barrier_semaphore()
+        for where in (to_x, to_y):
+            pl.semaphore_signal(barrier, inc=1, device_id=where, device_id_type=MESH)
+        pl.semaphore_wait(barrier, 2)
+        copies = []
+        for i in range(early, chunks):
+            a, b = pl.ds(i * size, size), pl.ds((i - early) * size, size)
+            for src, dst, where in (
+                (gp.at[0, a, :], lp_ref.at[b, :], to_y),
+                (go.at[1, :, a], lo_ref.at[:, b], to_x),
+            ):
+                c = pltpu.make_async_remote_copy(
+                    src_ref=src,
+                    dst_ref=dst,
+                    send_sem=out_s.at[len(copies)],
+                    recv_sem=out_r.at[len(copies)],
+                    device_id=where,
+                    device_id_type=MESH,
+                )
+                c.start()
+                copies.append(c)
+        for i in range(early, chunks - 1):
+            at = slice((i - early) * size, (i - early + 1) * size)
+            there = pl.ds(pl.multiple_of((3 - fs) * d_rows + i * size, size), size)
+            copies[2 * (i - early)].wait_recv()
+            u = proj_step(f_ref[0, there, :], d0_ref)
+            fp_ref[at, :] = (weight_of(lp_ref[at, :]) + u).astype(jnp.bfloat16)
+            copies[2 * (i - early) + 1].wait_recv()
+            u = out_step(f_ref[1, there, :], d1_ref)
+            fo_ref[:, at] = (weight_of(lo_ref[:, at]) + u).astype(jnp.bfloat16)
+        for c in copies[-2:]:
+            c.wait_recv()
+        for c in copies:
+            c.wait_send()
+
+
+def finish_kernel(
+    me_ref, core_ref, f_ref, d0, d1, lp, lo, fp, fo, pc_in, oc_in, pc_hbm, oc_hbm, last_p, last_o, sems
+):
+    me = me_ref[0]
+    d_rows = f_ref.shape[1] // 4
+    size = d_rows // chunks
+    done = fp.shape[0]
+
+    @pl.when(core_ref[0] == 0)
+    def _():
+        def span(start, n):
+            return pl.ds(pl.multiple_of((me ^ 3) * d_rows + start, size), n)
+
+        there = span(early * size, done)
+        copies = [
+            pltpu.make_async_copy(fp, pc_hbm.at[there, :], sems.at[0]),
+            pltpu.make_async_copy(fo, oc_hbm.at[:, there], sems.at[1]),
+        ]
+        for c in copies:
+            c.start()
+        there = span(d_rows - size, size)
+        u = proj_step(f_ref[0, there, :], d0)
+        last_p[...] = (weight_of(lp[done:, :]) + u).astype(jnp.bfloat16)
+        copies.append(pltpu.make_async_copy(last_p, pc_hbm.at[there, :], sems.at[2]))
+        copies[-1].start()
+        u = out_step(f_ref[1, there, :], d1)
+        last_o[...] = (weight_of(lo[:, done:]) + u).astype(jnp.bfloat16)
+        copies.append(pltpu.make_async_copy(last_o, oc_hbm.at[:, there], sems.at[3]))
+        copies[-1].start()
+        for c in copies:
+            c.wait()
 
 
 def fast_body(si, pc, sh, oc, factors, w_proj, w_out, m1, m2):
@@ -463,7 +600,7 @@
     quarter = width // 4
     args = (si, pc, sh, oc, factors, w_proj, w_out, mf, ms)
     held = tuple(pltpu.with_memory_space_constraint(a, pltpu.HBM) for a in args)
-    first, second, d0, d1, gp, go, pn, on, fp, fo = pl.pallas_call(
+    first, second, d0, d1, gp, go, pn, on, fp, fo, held_f = pl.pallas_call(
         functools.partial(exchange_kernel, tp_count, float(d_model * width * tp_count)),
         out_shape=(
             pltpu.VMEM((2 * rank, width), f32),
@@ -476,10 +613,11 @@
             pltpu.VMEM((width, d_rows), f32),
             pltpu.VMEM((4, d_rows, width), bf16),
             pltpu.VMEM((4, width, d_rows), bf16),
+            pltpu.VMEM(factors.shape, bf16),
         ),
         in_specs=[hbm] * 9,
-        out_specs=(vm,) * 10,
-        scratch_shapes=[pltpu.VMEM(a.shape, a.dtype) for a in args]
+        out_specs=(vm,) * 11,
+        scratch_shapes=[pltpu.VMEM(a.shape, a.dtype) for a in args if a is not factors]
         + [
             pltpu.VMEM((d_rows, width), bf16),
             pltpu.VMEM((width, d_rows), bf16),
@@ -509,9 +647,11 @@
     )(*held)
 
     me = lax.axis_index("fs").astype(jnp.int32).reshape(1)
+    core = lax.rem(lax.axis_index("tp"), 2).astype(jnp.int32).reshape(1)
+    scalar = pl.BlockSpec(memory_space=pltpu.SMEM)
     pn, on, pcopy, ocopy, first, second = pl.pallas_call(
-        finish_kernel,
-        in_specs=[pl.BlockSpec(memory_space=pltpu.SMEM)] + [vm] * 11,
+        write_kernel,
+        in_specs=[scalar] * 2 + [vm] * 6,
         out_specs=[hbm] * 6,
         out_shape=(
             shape(w_proj.shape, f32),
@@ -521,14 +661,40 @@
             shape((2 * rank, width), f32),
             shape((2 * rank, width), f32),
         ),
-        scratch_shapes=[
-            pltpu.VMEM((d_rows // chunks, width), bf16),
-            pltpu.VMEM((width, d_rows // chunks), bf16),
-            dma(14),
-        ],
-        compiler_params=pltpu.CompilerParams(vmem_limit_bytes=8 * MIB),
+        scratch_shapes=[dma(14)],
+        compiler_params=pltpu.CompilerParams(vmem_limit_bytes=4 * MIB),
+        name="write",
+    )(me, core, pn, on, fp, fo, first, second)
+
+    size = d_rows // chunks
+    late = chunks - early
+    lp, lo, fp, fo = pl.pallas_call(
+        relay_kernel,
+        in_specs=[vm] * 5,
+        out_specs=(vm,) * 4,
+        out_shape=(
+            pltpu.VMEM((late * size, width), bf16),
+            pltpu.VMEM((width, late * size), bf16),
+            pltpu.VMEM((late * size - size, width), bf16),
+            pltpu.VMEM((width, late * size - size), bf16),
+        ),
+        scratch_shapes=[dma(2 * late), dma(2 * late)],
+        compiler_params=pltpu.CompilerParams(
+            collective_id=1, has_side_effects=True, vmem_limit_bytes=8 * MIB
+        ),
+        name="relay",
+    )(held_f, d0, d1, gp, go)
+
+    pcopy, ocopy = pl.pallas_call(
+        finish_kernel,
+        in_specs=[scalar] * 2 + [vm] * 7 + [hbm] * 2,
+        out_specs=[hbm] * 2,
+        out_shape=(shape(pcopy.shape, bf16), shape(ocopy.shape, bf16)),
+        scratch_shapes=[pltpu.VMEM((size, width), bf16), pltpu.VMEM((width, size), bf16), dma(4)],
+        input_output_aliases={9: 0, 10: 1},
+        compiler_params=pltpu.CompilerParams(vmem_limit_bytes=4 * MIB),
         name="finish",
-    )(me, factors, d0, d1, gp, go, pn, on, fp, fo, first, second)
+    )(me, core, held_f, d0, d1, lp, lo, fp, fo, pcopy, ocopy)
     return pn, on, pcopy, ocopy, first.reshape(m1.shape), second.reshape(m2.shape)
 
 

time: 83.9 us -> 80.4 us (0.958)
  the two profiles are of different devices: /device:TPU:1 before, /device:TPU:0 now
where the time goes in v2:
time: 80.4 us; the launch traced here: 80.2 us
  Pallas kernels  79.6 us (99%)
    pallas_call x1, Pallas kernels, fast_body(): pl.pallas_call(functools.partial(exchange_kernel, tp_count, float(d_model...  61.4 us
    pallas_call x1, Pallas kernels, fast_body(): pl.pallas_call(relay_kernel, in_specs=[vm] * 5, out_specs=(vm,) * 4, out_...  12.5 us
    pallas_call x1, Pallas kernels, fast_body(): pl.pallas_call(write_kernel, in_specs=[scalar] * 2 + [vm] * 6, out_specs=...  4.5 us

profile of v2, /device:TPU:0, one launch (start us, length us, event | category | flops | bytes accessed | tf_op | source)
XLA Modules:
  0.0 80.2 jit_solution(17226404402136146239)
XLA Ops:
  0.6 61.4 %exchange.1 = (f32[256,512]{1,0:T(8,128)S(1)}, f32[256,512]{1,0:T(8,128)S(1)}, bf16[256,512]{1,0:T(8,128)(2,1)S(1)}, bf16[512,256]{1,0:T(8,128)(2,1)S(1)}, bf16[...) custom-call(bf16[672,512]{1,0:T(8,128)(2,1)} %si_hbm.1, ...), custom_call_target="tpu_custom_call" | custom-call | tf_op jit(solution)/shard_map/exchange/pallas_call | solution.py:603
  62.0 4.5 %write.1 = (f32[1024,512]{1,0:T(8,128)}, f32[512,1024]{1,0:T(8,128)}, bf16[4096,512]{1,0:T(8,128)(2,1)}, bf16[512,4096]{1,0:T(8,128)(2,1)}, f32[256,512]{1,0:T(8,128)}, /*index=5*/f32[256,512]{1,0:T(8,128)}) custom-call(s32[1]{0:T(128)} %bitcast.me_ref, s32[1]{0:T(128)} %bitcast.1.core_ref, f32[1024,512]{1,0:T(8,128)S(1)} %get-tuple-element.29.pn, ...), custom_call_target="tpu_custom_call" | custom-call | tf_op jit(solution)/shard_map/write/pallas_call | solution.py:652
  66.6 12.5 %relay.1 = (bf16[768,512]{1,0:T(8,128)(2,1)S(1)}, bf16[512,768]{1,0:T(8,128)(2,1)S(1)}, bf16[512,512]{1,0:T(8,128)(2,1)S(1)}, bf16[512,512]{1,0:T(8,128)(2,1)S(1)}) custom-call(bf16[2,4096,128]{2,1,0:T(8,128)(2,1)S(1)} %get-tuple-element.37.f_ref, bf16[256,512]{1,0:T(8,128)(2,1)S(1)} %get-tuple-element.38.d0_ref.d0, ...), custom_call_target="tpu_custom_call" | custom-call | tf_op jit(solution)/shard_map/relay/pallas_call | solution.py:671
  79.0 1.2 %finish.1 = (bf16[4096,512]{1,0:T(8,128)(2,1)}, bf16[512,4096]{1,0:T(8,128)(2,1)}) custom-call(s32[1]{0:T(128)} %bitcast.me_ref, s32[1]{0:T(128)} %bitcast.1.core_ref, bf16[2,4096,128]{2,1,0:T(8,128)(2,1)S(1)} %get-tuple-element.37.f_ref, bf16[256,512]{1,0:T(8,128)(2,1)S(1)} %get-tuple-element.38.d0_ref.d0, ...), custom_call_target="tpu_custom_call", output_to_operand_aliasing={{0}: (9, {}), {1}: (10, {})} | custom-call | tf_op jit(solution)/shard_map/finish/pallas_call | solution.py:688

commit v3 on v2

--- a/solution.py
+++ b/solution.py
@@ -15,8 +15,10 @@
 code_top = 200.0
 chunks = 4
 early = 1
+late_cuts = (4, 8, 12, 14, 16)
 pieces = 16
-pad_rows = 16
+pad_rows = 8
+lead = 1
 MIB = 1024 * 1024
 MESH = pl.DeviceIdType.MESH
 
@@ -117,6 +119,10 @@
     zin,
     zall,
     part,
+    pair_a,
+    pair_b,
+    pair_in_a,
+    pair_in_b,
     step_a,
     step_b,
     in_a,
@@ -169,12 +175,12 @@
 
     barrier = pltpu.get_barrier_semaphore()
 
-    @pl.when(core == 0)
+    @pl.when(core == lead)
     def _():
         signal(barrier, to_x)
         signal(barrier, to_y)
 
-    @pl.when(core == 1)
+    @pl.when(core != lead)
     def _():
         signal(barrier, {"tp": partner})
 
@@ -183,9 +189,9 @@
     def share(n, start, stop, of=chunks):
         return pl.ds(start * n // of, (stop - start) * n // of)
 
-    spans = ((0, 2), (2, 6), (6, 10), (10, 15))
+    spans = ((0, 1), (1, 5), (5, 10), (10, 15))
     pairs = []
-    for start, stop in (spans[0], (spans[0][1], pieces)):
+    for start, stop in (spans[0], spans[1], (spans[1][1], pieces)):
         a, b = share(d_rows, start, stop, pieces), share(width, start, stop, pieces)
         pairs += [(wp_hbm.at[a, :], wp_ref.at[a, :]), (wo_hbm.at[b, :], wo_ref.at[b, :])]
     pairs += [
@@ -223,13 +229,13 @@
     loads[1].wait()
     encode_out(*spans[0])
 
-    @pl.when(core == 0)
+    @pl.when(core == lead)
     def _():
         pl.semaphore_wait(barrier, 3)
         signal(known.at[0], to_x)
         signal(known.at[0], to_y)
 
-    @pl.when(core == 1)
+    @pl.when(core != lead)
     def _():
         pl.semaphore_wait(known.at[0], 1)
         for p in z_peers:
@@ -239,19 +245,22 @@
     open_out(*spans[0])
     for c in loads[4:]:
         c.start()
-
-    @pl.when(core == 0)
-    def _():
-        pl.semaphore_wait(known.at[0], 2)
-        signal(known.at[0], {"tp": partner})
-
-    loads[2].wait()
-    loads[3].wait()
-    for start, stop in spans[1:]:
+    for n, (start, stop) in enumerate(spans[1:]):
+        if n < 2:
+            loads[2 * n + 2].wait()
         encode_proj(start, stop)
         open_proj(start, stop)
+        if n < 2:
+            loads[2 * n + 3].wait()
         encode_out(start, stop)
         open_out(start, stop)
+        if n == 0:
+
+            @pl.when(core == lead)
+            def _():
+                pl.semaphore_wait(known.at[0], 2)
+                signal(known.at[0], {"tp": partner})
+
     last = spans[-1][1]
     encode_proj(last, pieces)
     encode_out(last, pieces)
@@ -262,7 +271,7 @@
         send(cp.at[a, :], gp_ref.at[1, a, :], to_y, 1, 3)
 
     cuts = (0, 1, 3, 5, 16)
-    for c in loads[4:7]:
+    for c in loads[6:9]:
         c.wait()
 
     tokens, feats = si_ref.shape
@@ -270,7 +279,7 @@
     rows[0] = jnp.dot(si_ref[...], f_ref[0, own, :], preferred_element_type=jnp.float32)
     rows[1] = jnp.dot(oc_ref[...], f_ref[1, own, :], preferred_element_type=jnp.float32)
     paired = send(rows.at[1 - core], pair_in, {"tp": partner}, 2, 4)
-    for c in loads[7:]:
+    for c in loads[9:]:
         c.wait()
     rank = f_ref.shape[2]
     grams = [
@@ -284,12 +293,12 @@
     def piece_of(i):
         return pl.ds(pl.multiple_of(i * piece, 8), piece)
 
-    @pl.when(core == 1)
+    @pl.when(core != lead)
     def _():
         pl.semaphore_wait(barrier, z_count - 1)
         signal(known.at[1], {"tp": partner})
 
-    @pl.when(core == 0)
+    @pl.when(core == lead)
     def _():
         pl.semaphore_wait(known.at[1], 1)
 
@@ -328,28 +337,26 @@
         for j in range(4):
             part[k, j] = both[:, j * width // 4 : (j + 1) * width // 4]
 
-    pack(step_a.at[0], part[0, across_x])
-    pack(step_a.at[1], part[0, diagonal])
-    pack(step_b.at[0], part[1, across_y])
-    pack(step_b.at[1], part[1, diagonal])
+    pack(pair_a, jnp.concatenate([part[0, across_x], part[0, diagonal]], axis=0))
+    pack(pair_b, jnp.concatenate([part[1, across_y], part[1, diagonal]], axis=0))
     sums = [
-        send(step_a.at[0:2], in_a.at[0:2], to_x, 3, 12),
-        send(step_b.at[0:2], in_b.at[0:2], to_y, 4, 13),
+        send(pair_a, pair_in_a, to_x, 3, 12),
+        send(pair_b, pair_in_b, to_y, 4, 13),
     ]
     open_proj(last, pieces)
     open_out(last, pieces)
     more(cuts[0], cuts[1])
     sums[0].wait_recv()
-    pack(step_a.at[2], part[0, across_y] + unpack(in_a.at[1], rank))
-    sums.append(send(step_a.at[2], in_a.at[2], to_y, 3, 14))
+    got_a = unpack(pair_in_a, 2 * rank)
+    pack(step_a, part[0, across_y] + got_a[rank:])
+    sums.append(send(step_a, in_a, to_y, 7, 14))
     sums[1].wait_recv()
-    pack(step_b.at[2], part[1, across_x] + unpack(in_b.at[1], rank))
-    sums.append(send(step_b.at[2], in_b.at[2], to_x, 4, 15))
+    got_b = unpack(pair_in_b, 2 * rank)
+    pack(step_b, part[1, across_x] + got_b[rank:])
+    sums.append(send(step_b, in_b, to_x, 8, 15))
     more(cuts[1], cuts[2])
-    mine_a = part[0, fs] + unpack(in_a.at[0], rank)
-    mine_b = part[1, fs] + unpack(in_b.at[0], rank)
     sums[2].wait_recv()
-    pack(quarters.at[0, fs], mine_a + unpack(in_a.at[2], rank))
+    pack(quarters.at[0, fs], part[0, fs] + got_a[:rank] + unpack(in_a, rank))
 
     def spread(k, at, where, r):
         return send(quarters.at[k, at], quarters.at[k, at], where, 5 + k, r)
@@ -357,7 +364,7 @@
     from_y = spread(0, fs, to_y, 16)
     spread(0, fs, to_x, 18)
     sums[3].wait_recv()
-    pack(quarters.at[1, fs], mine_b + unpack(in_b.at[2], rank))
+    pack(quarters.at[1, fs], part[1, fs] + got_b[:rank] + unpack(in_b, rank))
     from_x = spread(1, fs, to_x, 17)
     spread(1, fs, to_y, 18)
     more(cuts[2], cuts[3])
@@ -377,16 +384,16 @@
     for i in range(early):
         relay(i)
 
-    @pl.when(core == 1)
+    @pl.when(core != lead)
     def _():
         for i in range(early, chunks):
             relay(i)
 
     whole(quarters.at[0], 5, 18).wait_recv()
-    whole(step_a, 3, 12).wait_send()
-    whole(step_b, 4, 13).wait_send()
-    whole(step_a, 5, 12).wait_send()
-    whole(step_b, 6, 13).wait_send()
+    for c in sums:
+        c.wait_send()
+    whole(quarters.at[0, 0:3], 5, 12).wait_send()
+    whole(quarters.at[1, 0:3], 6, 13).wait_send()
 
     highest = lax.Precision.HIGHEST
     squares = []
@@ -454,7 +461,7 @@
     whole(gp_ref.at[2, a, :], 1, 0).wait_send()
     whole(go_ref.at[2, :, a], 0, 0).wait_send()
 
-    @pl.when(core == 1)
+    @pl.when(core != lead)
     def _():
         for i in range(early, chunks):
             relayed(i)
@@ -464,10 +471,11 @@
 
 
 def write_kernel(
-    me_ref, core_ref, pn, on, fp, fo, mf, ms,
-    pn_hbm, on_hbm, pc_hbm, oc_hbm, first_hbm, second_hbm, sems
+    pn, on, fp, fo, mf, ms,
+    pn_hbm, on_hbm, pc_hbm, oc_hbm, first_hbm, second_hbm, written, sems
 ):
-    me = me_ref[0]
+    me = lax.axis_index("fs")
+    core = lax.rem(lax.axis_index("tp"), 2)
     d_rows = pn.shape[0]
     size = d_rows // chunks
 
@@ -476,18 +484,18 @@
 
     def diagonal(start, stop):
         a = pl.ds(start * size, (stop - start) * size)
-        there = span(me ^ 3, start, stop)
+        there = span(3 - me, start, stop)
         return [(fp.at[3, a, :], pc_hbm.at[there, :]), (fo.at[3, :, a], oc_hbm.at[:, there])]
 
     pairs = [(pn, pn_hbm), (on, on_hbm), (mf, first_hbm), (ms, second_hbm)]
-    for r, owner in enumerate((me, me ^ 1, me ^ 2)):
+    for r, owner in enumerate((me, me + 1 - 2 * lax.rem(me, 2), lax.rem(me + 2, 4))):
         pairs += [(fp.at[r], pc_hbm.at[span(owner), :]), (fo.at[r], oc_hbm.at[:, span(owner)])]
     pairs += diagonal(0, early)
     copies = [pltpu.make_async_copy(a, b, sems.at[i]) for i, (a, b) in enumerate(pairs)]
     for c in copies:
         c.start()
 
-    @pl.when(core_ref[0] == 1)
+    @pl.when(core != lead)
     def _():
         rest = [
             pltpu.make_async_copy(a, b, sems.at[len(copies) + i])
@@ -500,25 +508,27 @@
 
     for c in copies:
         c.wait()
-
-
-def relay_kernel(f_ref, d0_ref, d1_ref, gp, go, lp_ref, lo_ref, fp_ref, fo_ref, out_s, out_r):
+    written[...] = jnp.zeros_like(written)
+
+
+def relay_kernel(written, f_ref, d0_ref, d1_ref, gp, go, lp_ref, lo_ref, fp_ref, fo_ref, out_s, out_r):
     fs = lax.axis_index("fs")
     core = lax.rem(lax.axis_index("tp"), 2)
     to_x = {"fs": fs + 1 - 2 * lax.rem(fs, 2)}
     to_y = {"fs": lax.rem(fs + 2, 4)}
     d_rows = gp.shape[1]
-    size = d_rows // chunks
-
-    @pl.when(core == 0)
+    first = early * d_rows // chunks
+
+    @pl.when(core == lead)
     def _():
         barrier = pltpu.get_barrier_semaphore()
         for where in (to_x, to_y):
             pl.semaphore_signal(barrier, inc=1, device_id=where, device_id_type=MESH)
         pl.semaphore_wait(barrier, 2)
         copies = []
-        for i in range(early, chunks):
-            a, b = pl.ds(i * size, size), pl.ds((i - early) * size, size)
+        for start, stop in zip(late_cuts[:-1], late_cuts[1:]):
+            start, stop = start * d_rows // pieces, stop * d_rows // pieces
+            a, b = pl.ds(start, stop - start), pl.ds(start - first, stop - start)
             for src, dst, where in (
                 (gp.at[0, a, :], lp_ref.at[b, :], to_y),
                 (go.at[1, :, a], lo_ref.at[:, b], to_x),
@@ -533,13 +543,14 @@
                 )
                 c.start()
                 copies.append(c)
-        for i in range(early, chunks - 1):
-            at = slice((i - early) * size, (i - early + 1) * size)
-            there = pl.ds(pl.multiple_of((3 - fs) * d_rows + i * size, size), size)
-            copies[2 * (i - early)].wait_recv()
+        for i, (start, stop) in enumerate(zip(late_cuts[:-2], late_cuts[1:-1])):
+            start, stop = start * d_rows // pieces, stop * d_rows // pieces
+            at = slice(start - first, stop - first)
+            there = pl.ds(pl.multiple_of((3 - fs) * d_rows + start, d_rows // pieces), stop - start)
+            copies[2 * i].wait_recv()
             u = proj_step(f_ref[0, there, :], d0_ref)
             fp_ref[at, :] = (weight_of(lp_ref[at, :]) + u).astype(jnp.bfloat16)
-            copies[2 * (i - early) + 1].wait_recv()
+            copies[2 * i + 1].wait_recv()
             u = out_step(f_ref[1, there, :], d1_ref)
             fo_ref[:, at] = (weight_of(lo_ref[:, at]) + u).astype(jnp.bfloat16)
         for c in copies[-2:]:
@@ -549,19 +560,19 @@
 
 
 def finish_kernel(
-    me_ref, core_ref, f_ref, d0, d1, lp, lo, fp, fo, pc_in, oc_in, pc_hbm, oc_hbm, last_p, last_o, sems
+    f_ref, d0, d1, lp, lo, fp, fo, pc_in, oc_in, pc_hbm, oc_hbm, last_p, last_o, sems
 ):
-    me = me_ref[0]
+    me = lax.axis_index("fs")
+    core = lax.rem(lax.axis_index("tp"), 2)
     d_rows = f_ref.shape[1] // 4
-    size = d_rows // chunks
-    done = fp.shape[0]
-
-    @pl.when(core_ref[0] == 0)
+    done, size = fp.shape[0], last_p.shape[0]
+
+    @pl.when(core == lead)
     def _():
         def span(start, n):
-            return pl.ds(pl.multiple_of((me ^ 3) * d_rows + start, size), n)
-
-        there = span(early * size, done)
+            return pl.ds(pl.multiple_of((3 - me) * d_rows + start, size), n)
+
+        there = span(d_rows - size - done, done)
         copies = [
             pltpu.make_async_copy(fp, pc_hbm.at[there, :], sems.at[0]),
             pltpu.make_async_copy(fo, oc_hbm.at[:, there], sems.at[1]),
@@ -577,7 +588,7 @@
         last_o[...] = (weight_of(lo[:, done:]) + u).astype(jnp.bfloat16)
         copies.append(pltpu.make_async_copy(last_o, oc_hbm.at[:, there], sems.at[3]))
         copies[-1].start()
-        for c in copies:
+        for i, c in enumerate(copies):
             c.wait()
 
 
@@ -628,16 +639,20 @@
             pltpu.VMEM((z_count - 1, packed, rank), bf16),
             pltpu.VMEM((2, z_count, packed, rank), bf16),
             pltpu.VMEM((2, 4, rank, quarter), f32),
-            pltpu.VMEM((3, rank + pad_rows, quarter), bf16),
-            pltpu.VMEM((3, rank + pad_rows, quarter), bf16),
-            pltpu.VMEM((3, rank + pad_rows, quarter), bf16),
-            pltpu.VMEM((3, rank + pad_rows, quarter), bf16),
+            pltpu.VMEM((2 * rank + pad_rows, quarter), bf16),
+            pltpu.VMEM((2 * rank + pad_rows, quarter), bf16),
+            pltpu.VMEM((2 * rank + pad_rows, quarter), bf16),
+            pltpu.VMEM((2 * rank + pad_rows, quarter), bf16),
+            pltpu.VMEM((rank + pad_rows, quarter), bf16),
+            pltpu.VMEM((rank + pad_rows, quarter), bf16),
+            pltpu.VMEM((rank + pad_rows, quarter), bf16),
+            pltpu.VMEM((rank + pad_rows, quarter), bf16),
             pltpu.VMEM((2, 4, rank + pad_rows, quarter), bf16),
             pltpu.VMEM((8, 128), f32),
             pltpu.VMEM((peers, 8, 128), f32),
             pltpu.SemaphoreType.REGULAR((2,)),
-            dma(11),
-            dma(7),
+            dma(13),
+            dma(9),
             dma(20 + 2 * chunks),
         ],
         compiler_params=pltpu.CompilerParams(
@@ -646,13 +661,10 @@
         name="exchange",
     )(*held)
 
-    me = lax.axis_index("fs").astype(jnp.int32).reshape(1)
-    core = lax.rem(lax.axis_index("tp"), 2).astype(jnp.int32).reshape(1)
-    scalar = pl.BlockSpec(memory_space=pltpu.SMEM)
-    pn, on, pcopy, ocopy, first, second = pl.pallas_call(
+    pn, on, pcopy, ocopy, first, second, written = pl.pallas_call(
         write_kernel,
-        in_specs=[scalar] * 2 + [vm] * 6,
-        out_specs=[hbm] * 6,
+        in_specs=[vm] * 6,
+        out_specs=[hbm] * 6 + [vm],
         out_shape=(
             shape(w_proj.shape, f32),
             shape(w_out.shape, f32),
@@ -660,41 +672,43 @@
             shape((width, d_model), bf16),
             shape((2 * rank, width), f32),
             shape((2 * rank, width), f32),
+            pltpu.VMEM((8, 128), f32),
         ),
         scratch_shapes=[dma(14)],
         compiler_params=pltpu.CompilerParams(vmem_limit_bytes=4 * MIB),
         name="write",
-    )(me, core, pn, on, fp, fo, first, second)
-
-    size = d_rows // chunks
-    late = chunks - early
+    )(pn, on, fp, fo, first, second)
+
+    size = d_rows * (late_cuts[-1] - late_cuts[-2]) // pieces
+    rest = d_rows - early * d_rows // chunks
+    count = 2 * len(late_cuts) - 2
     lp, lo, fp, fo = pl.pallas_call(
         relay_kernel,
-        in_specs=[vm] * 5,
+        in_specs=[vm] * 6,
         out_specs=(vm,) * 4,
         out_shape=(
-            pltpu.VMEM((late * size, width), bf16),
-            pltpu.VMEM((width, late * size), bf16),
-            pltpu.VMEM((late * size - size, width), bf16),
-            pltpu.VMEM((width, late * size - size), bf16),
+            pltpu.VMEM((rest, width), bf16),
+            pltpu.VMEM((width, rest), bf16),
+            pltpu.VMEM((rest - size, width), bf16),
+            pltpu.VMEM((width, rest - size), bf16),
         ),
-        scratch_shapes=[dma(2 * late), dma(2 * late)],
+        scratch_shapes=[dma(count), dma(count)],
         compiler_params=pltpu.CompilerParams(
             collective_id=1, has_side_effects=True, vmem_limit_bytes=8 * MIB
         ),
         name="relay",
-    )(held_f, d0, d1, gp, go)
+    )(written, held_f, d0, d1, gp, go)
 
     pcopy, ocopy = pl.pallas_call(
         finish_kernel,
-        in_specs=[scalar] * 2 + [vm] * 7 + [hbm] * 2,
+        in_specs=[vm] * 7 + [hbm] * 2,
         out_specs=[hbm] * 2,
         out_shape=(shape(pcopy.shape, bf16), shape(ocopy.shape, bf16)),
         scratch_shapes=[pltpu.VMEM((size, width), bf16), pltpu.VMEM((width, size), bf16), dma(4)],
-        input_output_aliases={9: 0, 10: 1},
+        input_output_aliases={7: 0, 8: 1},
         compiler_params=pltpu.CompilerParams(vmem_limit_bytes=4 * MIB),
         name="finish",
-    )(me, core, held_f, d0, d1, lp, lo, fp, fo, pcopy, ocopy)
+    )(held_f, d0, d1, lp, lo, fp, fo, pcopy, ocopy)
     return pn, on, pcopy, ocopy, first.reshape(m1.shape), second.reshape(m2.shape)
 
 

time: 80.4 us -> 78.3 us (0.974)
  the two profiles are of different devices: /device:TPU:0 before, /device:TPU:1 now
where the time goes in v3:
time: 78.3 us; the launch traced here: 78.1 us
  Pallas kernels  77.5 us (99%)
    pallas_call x1, Pallas kernels, fast_body(): pl.pallas_call(functools.partial(exchange_kernel, tp_count, float(d_model...  59.3 us
    pallas_call x1, Pallas kernels, fast_body(): pl.pallas_call(relay_kernel, in_specs=[vm] * 6, out_specs=(vm,) * 4, out_...  12.5 us
    pallas_call x1, Pallas kernels, fast_body(): pl.pallas_call(write_kernel, in_specs=[vm] * 6, out_specs=[hbm] * 6 + [vm...  4.5 us

profile of v3, /device:TPU:1, one launch (start us, length us, event | category | flops | bytes accessed | tf_op | source)
XLA Modules:
  0.0 78.1 jit_solution(14475325511649098622)
XLA Ops:
  0.6 59.3 %exchange.1 = (f32[256,512]{1,0:T(8,128)S(1)}, f32[256,512]{1,0:T(8,128)S(1)}, bf16[256,512]{1,0:T(8,128)(2,1)S(1)}, bf16[512,256]{1,0:T(8,128)(2,1)S(1)}, bf16[...) custom-call(bf16[672,512]{1,0:T(8,128)(2,1)} %si_hbm.1, ...), custom_call_target="tpu_custom_call" | custom-call | tf_op jit(solution)/shard_map/exchange/pallas_call | solution.py:614
  59.9 4.5 %write.1 = (f32[1024,512]{1,0:T(8,128)}, f32[512,1024]{1,0:T(8,128)}, bf16[4096,512]{1,0:T(8,128)(2,1)}, bf16[512,4096]{1,0:T(8,128)(2,1)}, f32[256,512]{1,0:T(8...) custom-call(f32[1024,512]{1,0:T(8,128)S(1)} %get-tuple-element.30.pn, f32[512,1024]{1,0:T(8,128)S(1)} %get-tuple-element.31.on, ...), custom_call_target="tpu_custom_call" | custom-call | tf_op jit(solution)/shard_map/write/pallas_call | solution.py:664
  64.4 12.5 %relay.1 = (bf16[768,512]{1,0:T(8,128)(2,1)S(1)}, bf16[512,768]{1,0:T(8,128)(2,1)S(1)}, bf16[640,512]{1,0:T(8,128)(2,1)S(1)}, bf16[512,640]{1,0:T(8,128)(2,1)S(1)}) custom-call(f32[8,128]{1,0:T(8,128)S(1)} %get-tuple-element.41.written, bf16[2,4096,128]{2,1,0:T(8,128)(2,1)S(1)} %get-tuple-element.38.f_ref, bf16[256,512]{1,0:T(8,128)(2,1)S(1)} %get-tuple-element.39.d0_ref.d0, ...), custom_call_target="tpu_custom_call" | custom-call | tf_op jit(solution)/shard_map/relay/pallas_call | solution.py:685
  76.9 1.2 %finish.1 = (bf16[4096,512]{1,0:T(8,128)(2,1)}, bf16[512,4096]{1,0:T(8,128)(2,1)}) custom-call(bf16[2,4096,128]{2,1,0:T(8,128)(2,1)S(1)} %get-tuple-element.38.f_ref, bf16[256,512]{1,0:T(8,128)(2,1)S(1)} %get-tuple-element.39.d0_ref.d0, bf16[512,256]{1,0:T(8,128)(2,1)S(1)} %get-tuple-element.40.d1_ref.d1, ...), custom_call_target="tpu_custom_call", output_to_operand_aliasing={{0}: (7, {}), {1}: (8, {})} | custom-call | tf_op jit(solution)/shard_map/finish/pallas_call | solution.py:702

commit v4 on v3

--- a/solution.py
+++ b/solution.py
@@ -11,7 +11,7 @@
 beta_second = 0.95
 learn_rate = 0.02
 epsilon = 1e-06
-weight_rate = 1344.0
+weight_rate = 1328.0
 code_top = 200.0
 chunks = 4
 early = 1
@@ -175,21 +175,12 @@
 
     barrier = pltpu.get_barrier_semaphore()
 
-    @pl.when(core == lead)
-    def _():
-        signal(barrier, to_x)
-        signal(barrier, to_y)
-
-    @pl.when(core != lead)
-    def _():
-        signal(barrier, {"tp": partner})
-
     d_rows, width = cp.shape
 
     def share(n, start, stop, of=chunks):
         return pl.ds(start * n // of, (stop - start) * n // of)
 
-    spans = ((0, 1), (1, 5), (5, 10), (10, 15))
+    spans = ((0, 2), (2, 6), (6, 10), (10, 15))
     pairs = []
     for start, stop in (spans[0], spans[1], (spans[1][1], pieces)):
         a, b = share(d_rows, start, stop, pieces), share(width, start, stop, pieces)
@@ -204,7 +195,29 @@
         (ms_hbm, ms_ref),
     ]
     loads = [pltpu.make_async_copy(a, b, in_s.at[i]) for i, (a, b) in enumerate(pairs)]
-    for c in loads[:4]:
+    for c in loads[:2]:
+        c.start()
+
+    at_x, at_y = lax.rem(fs, 2), fs // 2
+
+    @pl.when(jnp.logical_and(core == lead, at_x == 0))
+    def _():
+        signal(barrier, to_x)
+
+    @pl.when(jnp.logical_and(core == lead, at_y == 0))
+    def _():
+        signal(barrier, to_y)
+
+    @pl.when(core == lead)
+    def _():
+        signal(barrier, {"tp": partner})
+
+    @pl.when(core != lead)
+    def _():
+        for p in z_peers:
+            signal(barrier, {"tp": p})
+
+    for c in loads[2:4]:
         c.start()
 
 
@@ -223,43 +236,80 @@
     def open_out(start, stop):
         b = share(width, start, stop, pieces)
         send(co.at[b, :], go_ref.at[1, b, :], to_y, 1, 1)
+
+    @pl.when(jnp.logical_and(core == lead, fs > 0))
+    def _():
+        pl.semaphore_wait(barrier, at_x + at_y)
+
+    @pl.when(jnp.logical_and(core == lead, at_x == 1))
+    def _():
+        signal(known.at[2], to_x)
+
+    @pl.when(jnp.logical_and(core == lead, at_y == 1))
+    def _():
+        signal(known.at[3], to_y)
 
     loads[0].wait()
     encode_proj(*spans[0])
     loads[1].wait()
     encode_out(*spans[0])
 
-    @pl.when(core == lead)
-    def _():
-        pl.semaphore_wait(barrier, 3)
-        signal(known.at[0], to_x)
-        signal(known.at[0], to_y)
-
-    @pl.when(core != lead)
-    def _():
-        pl.semaphore_wait(known.at[0], 1)
-        for p in z_peers:
-            signal(barrier, {"tp": p})
-
-    open_proj(*spans[0])
-    open_out(*spans[0])
+    def first_x():
+        @pl.when(at_x == 0)
+        def _():
+            pl.semaphore_wait(known.at[2], 1)
+
+        open_proj(*spans[0])
+
+    def first_y():
+        @pl.when(at_y == 0)
+        def _():
+            pl.semaphore_wait(known.at[3], 1)
+
+        open_out(*spans[0])
+
+    @pl.when(jnp.logical_and(core == lead, at_x >= at_y))
+    def _():
+        first_x()
+        first_y()
+
+    @pl.when(jnp.logical_and(core == lead, at_x < at_y))
+    def _():
+        first_y()
+        first_x()
+
     for c in loads[4:]:
         c.start()
     for n, (start, stop) in enumerate(spans[1:]):
         if n < 2:
             loads[2 * n + 2].wait()
+            loads[2 * n + 3].wait()
         encode_proj(start, stop)
-        open_proj(start, stop)
-        if n < 2:
-            loads[2 * n + 3].wait()
         encode_out(start, stop)
-        open_out(start, stop)
-        if n == 0:
-
-            @pl.when(core == lead)
-            def _():
-                pl.semaphore_wait(known.at[0], 2)
-                signal(known.at[0], {"tp": partner})
+
+        @pl.when(core == lead)
+        def _(start=start, stop=stop):
+            open_proj(start, stop)
+            open_out(start, stop)
+
+
+    @pl.when(core == lead)
+    def _():
+        pl.semaphore_wait(known.at[1], 1)
+        signal(known.at[0], to_x)
+        signal(known.at[0], to_y)
+        pl.semaphore_wait(known.at[0], 2)
+        signal(known.at[0], {"tp": partner})
+
+    @pl.when(core != lead)
+    def _():
+        pl.semaphore_wait(barrier, z_count)
+        signal(known.at[1], {"tp": partner})
+        for p in z_peers:
+            signal(known.at[1], {"tp": p})
+        pl.semaphore_wait(known.at[0], 1)
+        open_proj(0, spans[-1][1])
+        open_out(0, spans[-1][1])
 
     last = spans[-1][1]
     encode_proj(last, pieces)
@@ -270,7 +320,7 @@
         send(co.at[b, :], go_ref.at[0, b, :], to_x, 0, 2)
         send(cp.at[a, :], gp_ref.at[1, a, :], to_y, 1, 3)
 
-    cuts = (0, 1, 3, 5, 16)
+    cuts = (0, 2, 5, 8, 16)
     for c in loads[6:9]:
         c.wait()
 
@@ -295,12 +345,12 @@
 
     @pl.when(core != lead)
     def _():
-        pl.semaphore_wait(barrier, z_count - 1)
-        signal(known.at[1], {"tp": partner})
+        pl.semaphore_wait(known.at[1], z_count - 1)
+        signal(known.at[4], {"tp": partner})
 
     @pl.when(core == lead)
     def _():
-        pl.semaphore_wait(known.at[1], 1)
+        pl.semaphore_wait(known.at[4], 1)
 
     scatter = []
     for i, p in enumerate(z_peers):
@@ -536,7 +586,7 @@
                 c = pltpu.make_async_remote_copy(
                     src_ref=src,
                     dst_ref=dst,
-                    send_sem=out_s.at[len(copies)],
+                    send_sem=out_s.at[len(copies) % 2],
                     recv_sem=out_r.at[len(copies)],
                     device_id=where,
                     device_id_type=MESH,
@@ -555,8 +605,15 @@
             fo_ref[:, at] = (weight_of(lo_ref[:, at]) + u).astype(jnp.bfloat16)
         for c in copies[-2:]:
             c.wait_recv()
-        for c in copies:
-            c.wait_send()
+        for i, ref in enumerate((lp_ref, lo_ref)):
+            pltpu.make_async_remote_copy(
+                src_ref=ref,
+                dst_ref=ref,
+                send_sem=out_s.at[i],
+                recv_sem=out_r.at[i],
+                device_id=to_x,
+                device_id_type=MESH,
+            ).wait_send()
 
 
 def finish_kernel(
@@ -566,6 +623,7 @@
     core = lax.rem(lax.axis_index("tp"), 2)
     d_rows = f_ref.shape[1] // 4
     done, size = fp.shape[0], last_p.shape[0]
+    half = fo.shape[0] // 2
 
     @pl.when(core == lead)
     def _():
@@ -575,19 +633,22 @@
         there = span(d_rows - size - done, done)
         copies = [
             pltpu.make_async_copy(fp, pc_hbm.at[there, :], sems.at[0]),
-            pltpu.make_async_copy(fo, oc_hbm.at[:, there], sems.at[1]),
+            pltpu.make_async_copy(fo.at[:half, :], oc_hbm.at[:half, there], sems.at[1]),
+            pltpu.make_async_copy(fo.at[half:, :], oc_hbm.at[half:, there], sems.at[4]),
         ]
         for c in copies:
             c.start()
         there = span(d_rows - size, size)
         u = proj_step(f_ref[0, there, :], d0)
+        v = out_step(f_ref[1, there, :], d1)
         last_p[...] = (weight_of(lp[done:, :]) + u).astype(jnp.bfloat16)
-        copies.append(pltpu.make_async_copy(last_p, pc_hbm.at[there, :], sems.at[2]))
-        copies[-1].start()
-        u = out_step(f_ref[1, there, :], d1)
-        last_o[...] = (weight_of(lo[:, done:]) + u).astype(jnp.bfloat16)
-        copies.append(pltpu.make_async_copy(last_o, oc_hbm.at[:, there], sems.at[3]))
-        copies[-1].start()
+        last_o[...] = (weight_of(lo[:, done:]) + v).astype(jnp.bfloat16)
+        copies += [
+            pltpu.make_async_copy(last_p, pc_hbm.at[there, :], sems.at[2]),
+            pltpu.make_async_copy(last_o, oc_hbm.at[:, there], sems.at[3]),
+        ]
+        for c in copies[3:]:
+            c.start()
         for i, c in enumerate(copies):
             c.wait()
 
@@ -650,7 +711,7 @@
             pltpu.VMEM((2, 4, rank + pad_rows, quarter), bf16),
             pltpu.VMEM((8, 128), f32),
             pltpu.VMEM((peers, 8, 128), f32),
-            pltpu.SemaphoreType.REGULAR((2,)),
+            pltpu.SemaphoreType.REGULAR((5,)),
             dma(13),
             dma(9),
             dma(20 + 2 * chunks),
@@ -692,7 +753,7 @@
             pltpu.VMEM((rest - size, width), bf16),
             pltpu.VMEM((width, rest - size), bf16),
         ),
-        scratch_shapes=[dma(count), dma(count)],
+        scratch_shapes=[dma(2), dma(count)],
         compiler_params=pltpu.CompilerParams(
             collective_id=1, has_side_effects=True, vmem_limit_bytes=8 * MIB
         ),
@@ -704,7 +765,7 @@
         in_specs=[vm] * 7 + [hbm] * 2,
         out_specs=[hbm] * 2,
         out_shape=(shape(pcopy.shape, bf16), shape(ocopy.shape, bf16)),
-        scratch_shapes=[pltpu.VMEM((size, width), bf16), pltpu.VMEM((width, size), bf16), dma(4)],
+        scratch_shapes=[pltpu.VMEM((size, width), bf16), pltpu.VMEM((width, size), bf16), dma(5)],
         input_output_aliases={7: 0, 8: 1},
         compiler_params=pltpu.CompilerParams(vmem_limit_bytes=4 * MIB),
         name="finish",

time: 78.3 us -> 78.2 us (level)
    pallas_call x1, Pallas kernels: 12.5 us -> 11.5 us  [fast_body(): pl.pallas_call(relay_kernel, in_specs=[vm] * 6, out_specs=(vm,) * 4, out_...]
where the time goes in v4:
time: 78.2 us; the launch traced here: 78.1 us
  Pallas kernels  77.4 us (99%)
    pallas_call x1, Pallas kernels, fast_body(): pl.pallas_call(functools.partial(exchange_kernel, tp_count, float(d_model...  60 us
    pallas_call x1, Pallas kernels, fast_body(): pl.pallas_call(relay_kernel, in_specs=[vm] * 6, out_specs=(vm,) * 4, out_...  11.5 us
    pallas_call x1, Pallas kernels, fast_body(): pl.pallas_call(write_kernel, in_specs=[vm] * 6, out_specs=[hbm] * 6 + [vm...  4.5 us

profile of v4, /device:TPU:1, one launch (start us, length us, event | category | flops | bytes accessed | tf_op | source)
XLA Modules:
  0.0 78.1 jit_solution(15897797805092829204)
XLA Ops:
  0.6 60.0 %exchange.1 = (f32[256,512]{1,0:T(8,128)S(1)}, f32[256,512]{1,0:T(8,128)S(1)}, bf16[256,512]{1,0:T(8,128)(2,1)S(1)}, bf16[512,256]{1,0:T(8,128)(2,1)S(1)}, bf16[...) custom-call(bf16[672,512]{1,0:T(8,128)(2,1)} %si_hbm.1, ...), custom_call_target="tpu_custom_call" | custom-call | tf_op jit(solution)/shard_map/exchange/pallas_call | solution.py:675
  60.6 4.5 %write.1 = (f32[1024,512]{1,0:T(8,128)}, f32[512,1024]{1,0:T(8,128)}, bf16[4096,512]{1,0:T(8,128)(2,1)}, bf16[512,4096]{1,0:T(8,128)(2,1)}, f32[256,512]{1,0:T(8...) custom-call(f32[1024,512]{1,0:T(8,128)S(1)} %get-tuple-element.30.pn, f32[512,1024]{1,0:T(8,128)S(1)} %get-tuple-element.31.on, ...), custom_call_target="tpu_custom_call" | custom-call | tf_op jit(solution)/shard_map/write/pallas_call | solution.py:725
  65.1 11.5 %relay.1 = (bf16[768,512]{1,0:T(8,128)(2,1)S(1)}, bf16[512,768]{1,0:T(8,128)(2,1)S(1)}, bf16[640,512]{1,0:T(8,128)(2,1)S(1)}, bf16[512,640]{1,0:T(8,128)(2,1)S(1)}) custom-call(f32[8,128]{1,0:T(8,128)S(1)} %get-tuple-element.41.written, bf16[2,4096,128]{2,1,0:T(8,128)(2,1)S(1)} %get-tuple-element.38.f_ref, bf16[256,512]{1,0:T(8,128)(2,1)S(1)} %get-tuple-element.39.d0_ref.d0, ...), custom_call_target="tpu_custom_call" | custom-call | tf_op jit(solution)/shard_map/relay/pallas_call | solution.py:746
  76.7 1.4 %finish.1 = (bf16[4096,512]{1,0:T(8,128)(2,1)}, bf16[512,4096]{1,0:T(8,128)(2,1)}) custom-call(bf16[2,4096,128]{2,1,0:T(8,128)(2,1)S(1)} %get-tuple-element.38.f_ref, bf16[256,512]{1,0:T(8,128)(2,1)S(1)} %get-tuple-element.39.d0_ref.d0, bf16[512,256]{1,0:T(8,128)(2,1)S(1)} %get-tuple-element.40.d1_ref.d1, ...), custom_call_target="tpu_custom_call", output_to_operand_aliasing={{0}: (7, {}), {1}: (8, {})} | custom-call | tf_op jit(solution)/shard_map/finish/pallas_call | solution.py:763

commit v5 on v4

--- a/solution.py
+++ b/solution.py
@@ -561,7 +561,9 @@
     written[...] = jnp.zeros_like(written)
 
 
-def relay_kernel(written, f_ref, d0_ref, d1_ref, gp, go, lp_ref, lo_ref, fp_ref, fo_ref, out_s, out_r):
+def relay_kernel(
+    written, f_ref, d0_ref, d1_ref, gp, go, lp_ref, lo_ref, fp_ref, fo_ref, up_ref, uo_ref, out_s, out_r
+):
     fs = lax.axis_index("fs")
     core = lax.rem(lax.axis_index("tp"), 2)
     to_x = {"fs": fs + 1 - 2 * lax.rem(fs, 2)}
@@ -593,6 +595,10 @@
                 )
                 c.start()
                 copies.append(c)
+        last = d_rows - up_ref.shape[0]
+        there = pl.ds(pl.multiple_of((3 - fs) * d_rows + last, up_ref.shape[0]), up_ref.shape[0])
+        up_ref[...] = proj_step(f_ref[0, there, :], d0_ref)
+        uo_ref[...] = out_step(f_ref[1, there, :], d1_ref)
         for i, (start, stop) in enumerate(zip(late_cuts[:-2], late_cuts[1:-1])):
             start, stop = start * d_rows // pieces, stop * d_rows // pieces
             at = slice(start - first, stop - first)
@@ -616,14 +622,11 @@
             ).wait_send()
 
 
-def finish_kernel(
-    f_ref, d0, d1, lp, lo, fp, fo, pc_in, oc_in, pc_hbm, oc_hbm, last_p, last_o, sems
-):
+def finish_kernel(lp, lo, fp, fo, up, uo, pc_in, oc_in, pc_hbm, oc_hbm, last_p, last_o, sems):
     me = lax.axis_index("fs")
     core = lax.rem(lax.axis_index("tp"), 2)
-    d_rows = f_ref.shape[1] // 4
+    d_rows = pc_hbm.shape[0] // 4
     done, size = fp.shape[0], last_p.shape[0]
-    half = fo.shape[0] // 2
 
     @pl.when(core == lead)
     def _():
@@ -633,22 +636,17 @@
         there = span(d_rows - size - done, done)
         copies = [
             pltpu.make_async_copy(fp, pc_hbm.at[there, :], sems.at[0]),
-            pltpu.make_async_copy(fo.at[:half, :], oc_hbm.at[:half, there], sems.at[1]),
-            pltpu.make_async_copy(fo.at[half:, :], oc_hbm.at[half:, there], sems.at[4]),
+            pltpu.make_async_copy(fo, oc_hbm.at[:, there], sems.at[1]),
         ]
         for c in copies:
             c.start()
         there = span(d_rows - size, size)
-        u = proj_step(f_ref[0, there, :], d0)
-        v = out_step(f_ref[1, there, :], d1)
-        last_p[...] = (weight_of(lp[done:, :]) + u).astype(jnp.bfloat16)
-        last_o[...] = (weight_of(lo[:, done:]) + v).astype(jnp.bfloat16)
-        copies += [
-            pltpu.make_async_copy(last_p, pc_hbm.at[there, :], sems.at[2]),
-            pltpu.make_async_copy(last_o, oc_hbm.at[:, there], sems.at[3]),
-        ]
-        for c in copies[3:]:
-            c.start()
+        last_p[...] = (weight_of(lp[done:, :]) + up[...]).astype(jnp.bfloat16)
+        copies.append(pltpu.make_async_copy(last_p, pc_hbm.at[there, :], sems.at[2]))
+        copies[-1].start()
+        last_o[...] = (weight_of(lo[:, done:]) + uo[...]).astype(jnp.bfloat16)
+        copies.append(pltpu.make_async_copy(last_o, oc_hbm.at[:, there], sems.at[3]))
+        copies[-1].start()
         for i, c in enumerate(copies):
             c.wait()
 
@@ -743,15 +741,17 @@
     size = d_rows * (late_cuts[-1] - late_cuts[-2]) // pieces
     rest = d_rows - early * d_rows // chunks
     count = 2 * len(late_cuts) - 2
-    lp, lo, fp, fo = pl.pallas_call(
+    lp, lo, fp, fo, up, uo = pl.pallas_call(
         relay_kernel,
         in_specs=[vm] * 6,
-        out_specs=(vm,) * 4,
+        out_specs=(vm,) * 6,
         out_shape=(
             pltpu.VMEM((rest, width), bf16),
             pltpu.VMEM((width, rest), bf16),
             pltpu.VMEM((rest - size, width), bf16),
             pltpu.VMEM((width, rest - size), bf16),
+            pltpu.VMEM((size, width), f32),
+            pltpu.VMEM((width, size), f32),
         ),
         scratch_shapes=[dma(2), dma(count)],
         compiler_params=pltpu.CompilerParams(
@@ -762,14 +762,14 @@
 
     pcopy, ocopy = pl.pallas_call(
         finish_kernel,
-        in_specs=[vm] * 7 + [hbm] * 2,
+        in_specs=[vm] * 6 + [hbm] * 2,
         out_specs=[hbm] * 2,
         out_shape=(shape(pcopy.shape, bf16), shape(ocopy.shape, bf16)),
-        scratch_shapes=[pltpu.VMEM((size, width), bf16), pltpu.VMEM((width, size), bf16), dma(5)],
-        input_output_aliases={7: 0, 8: 1},
+        scratch_shapes=[pltpu.VMEM((size, width), bf16), pltpu.VMEM((width, size), bf16), dma(4)],
+        input_output_aliases={6: 0, 7: 1},
         compiler_params=pltpu.CompilerParams(vmem_limit_bytes=4 * MIB),
         name="finish",
-    )(held_f, d0, d1, lp, lo, fp, fo, pcopy, ocopy)
+    )(lp, lo, fp, fo, up, uo, pcopy, ocopy)
     return pn, on, pcopy, ocopy, first.reshape(m1.shape), second.reshape(m2.shape)
 
 

time: 78.2 us -> 78 us (level)
  no operation moved by 1% of the time
where the time goes in v5:
time: 78 us; the launch traced here: 77.9 us
  Pallas kernels  77.2 us (99%)
    pallas_call x1, Pallas kernels, fast_body(): pl.pallas_call(functools.partial(exchange_kernel, tp_count, float(d_model...  60 us
    pallas_call x1, Pallas kernels, fast_body(): pl.pallas_call(relay_kernel, in_specs=[vm] * 6, out_specs=(vm,) * 6, out_...  11.5 us
    pallas_call x1, Pallas kernels, fast_body(): pl.pallas_call(write_kernel, in_specs=[vm] * 6, out_specs=[hbm] * 6 + [vm...  4.5 us

profile of v5, /device:TPU:1, one launch (start us, length us, event | category | flops | bytes accessed | tf_op | source)
XLA Modules:
  0.0 77.9 jit_solution(1135185922367963694)
XLA Ops:
  0.6 60.0 %exchange.1 = (f32[256,512]{1,0:T(8,128)S(1)}, f32[256,512]{1,0:T(8,128)S(1)}, bf16[256,512]{1,0:T(8,128)(2,1)S(1)}, bf16[512,256]{1,0:T(8,128)(2,1)S(1)}, bf16[...) custom-call(bf16[672,512]{1,0:T(8,128)(2,1)} %si_hbm.1, ...), custom_call_target="tpu_custom_call" | custom-call | tf_op jit(solution)/shard_map/exchange/pallas_call | solution.py:673
  60.6 4.5 %write.1 = (f32[1024,512]{1,0:T(8,128)}, f32[512,1024]{1,0:T(8,128)}, bf16[4096,512]{1,0:T(8,128)(2,1)}, bf16[512,4096]{1,0:T(8,128)(2,1)}, f32[256,512]{1,0:T(8...) custom-call(f32[1024,512]{1,0:T(8,128)S(1)} %get-tuple-element.32.pn, f32[512,1024]{1,0:T(8,128)S(1)} %get-tuple-element.33.on, ...), custom_call_target="tpu_custom_call" | custom-call | tf_op jit(solution)/shard_map/write/pallas_call | solution.py:723
  65.1 11.5 %relay.1 = (bf16[768,512]{1,0:T(8,128)(2,1)S(1)}, bf16[512,768]{1,0:T(8,128)(2,1)S(1)}, bf16[640,512]{1,0:T(8,128)(2,1)S(1)}, bf16[512,640]{1,0:T(8,128)(2,1)S(1...) custom-call(f32[8,128]{1,0:T(8,128)S(1)} %get-tuple-element.40.written, ...), custom_call_target="tpu_custom_call" | custom-call | tf_op jit(solution)/shard_map/relay/pallas_call | solution.py:744
  76.7 1.2 %finish.1 = (bf16[4096,512]{1,0:T(8,128)(2,1)}, bf16[512,4096]{1,0:T(8,128)(2,1)}) custom-call(bf16[768,512]{1,0:T(8,128)(2,1)S(1)} %get-tuple-element.46.lp, bf16[512,768]{1,0:T(8,128)(2,1)S(1)} %get-tuple-element.47.lo, bf16[640,512]{1,0:T(8,128)(2,1)S(1)} %get-tuple-element.48.fp, ...), custom_call_target="tpu_custom_call", output_to_operand_aliasing={{0}: (6, {}), {1}: (7, {})} | custom-call | tf_op jit(solution)/shard_map/finish/pallas_call | solution.py:763

commit v6 on v5

--- a/solution.py
+++ b/solution.py
@@ -249,12 +249,11 @@
     def _():
         signal(known.at[3], to_y)
 
-    loads[0].wait()
-    encode_proj(*spans[0])
-    loads[1].wait()
-    encode_out(*spans[0])
 
     def first_x():
+        loads[0].wait()
+        encode_proj(*spans[0])
+
         @pl.when(at_x == 0)
         def _():
             pl.semaphore_wait(known.at[2], 1)
@@ -262,11 +261,21 @@
         open_proj(*spans[0])
 
     def first_y():
+        loads[1].wait()
+        encode_out(*spans[0])
+
         @pl.when(at_y == 0)
         def _():
             pl.semaphore_wait(known.at[3], 1)
 
         open_out(*spans[0])
+
+    @pl.when(core != lead)
+    def _():
+        loads[0].wait()
+        encode_proj(*spans[0])
+        loads[1].wait()
+        encode_out(*spans[0])
 
     @pl.when(jnp.logical_and(core == lead, at_x >= at_y))
     def _():

time: 78 us -> 78 us (level)
  no operation moved by 1% of the time
where the time goes in v6:
time: 78 us; the launch traced here: 77.9 us
  Pallas kernels  77.2 us (99%)
    pallas_call x1, Pallas kernels, fast_body(): pl.pallas_call(functools.partial(exchange_kernel, tp_count, float(d_model...  60 us
    pallas_call x1, Pallas kernels, fast_body(): pl.pallas_call(relay_kernel, in_specs=[vm] * 6, out_specs=(vm,) * 6, out_...  11.5 us
    pallas_call x1, Pallas kernels, fast_body(): pl.pallas_call(write_kernel, in_specs=[vm] * 6, out_specs=[hbm] * 6 + [vm...  4.5 us

profile of v6, /device:TPU:1, one launch (start us, length us, event | category | flops | bytes accessed | tf_op | source)
XLA Modules:
  0.0 77.9 jit_solution(12136887864435584108)
XLA Ops:
  0.6 60.0 %exchange.1 = (f32[256,512]{1,0:T(8,128)S(1)}, f32[256,512]{1,0:T(8,128)S(1)}, bf16[256,512]{1,0:T(8,128)(2,1)S(1)}, bf16[512,256]{1,0:T(8,128)(2,1)S(1)}, bf16[...) custom-call(bf16[672,512]{1,0:T(8,128)(2,1)} %si_hbm.1, ...), custom_call_target="tpu_custom_call" | custom-call | tf_op jit(solution)/shard_map/exchange/pallas_call | solution.py:682
  60.6 4.5 %write.1 = (f32[1024,512]{1,0:T(8,128)}, f32[512,1024]{1,0:T(8,128)}, bf16[4096,512]{1,0:T(8,128)(2,1)}, bf16[512,4096]{1,0:T(8,128)(2,1)}, f32[256,512]{1,0:T(8...) custom-call(f32[1024,512]{1,0:T(8,128)S(1)} %get-tuple-element.32.pn, f32[512,1024]{1,0:T(8,128)S(1)} %get-tuple-element.33.on, ...), custom_call_target="tpu_custom_call" | custom-call | tf_op jit(solution)/shard_map/write/pallas_call | solution.py:732
  65.1 11.5 %relay.1 = (bf16[768,512]{1,0:T(8,128)(2,1)S(1)}, bf16[512,768]{1,0:T(8,128)(2,1)S(1)}, bf16[640,512]{1,0:T(8,128)(2,1)S(1)}, bf16[512,640]{1,0:T(8,128)(2,1)S(1...) custom-call(f32[8,128]{1,0:T(8,128)S(1)} %get-tuple-element.40.written, ...), custom_call_target="tpu_custom_call" | custom-call | tf_op jit(solution)/shard_map/relay/pallas_call | solution.py:753
  76.7 1.2 %finish.1 = (bf16[4096,512]{1,0:T(8,128)(2,1)}, bf16[512,4096]{1,0:T(8,128)(2,1)}) custom-call(bf16[768,512]{1,0:T(8,128)(2,1)S(1)} %get-tuple-element.46.lp, bf16[512,768]{1,0:T(8,128)(2,1)S(1)} %get-tuple-element.47.lo, bf16[640,512]{1,0:T(8,128)(2,1)S(1)} %get-tuple-element.48.fp, ...), custom_call_target="tpu_custom_call", output_to_operand_aliasing={{0}: (6, {}), {1}: (7, {})} | custom-call | tf_op jit(solution)/shard_map/finish/pallas_call | solution.py:772
